TPU v7x, 32 devices: a whole 2x2x4 slice. The times are simulated.
32 devices in a mesh: sp: 4 (over y, x), tp: 8 (over z, core).
Axes of the slice: x: 2, y: 2, z: 4, core: 2. Of those that a mesh axis runs over, the one named last changes fastest.
Arguments:
- residual_mid: bfloat16 [640, 4096], P('sp'), may hold values from -100 to 100
- out_grad: bfloat16 [640, 4096], P('sp'), may hold values from -6 to 6
- norm_gain: float32 [4096], replicated, may hold values from 0.1 to 1.9
- expert_ids: int32 [640, 2], P('sp'), may hold values from 0 to 3, all different within a row; in each aligned block of 160 rows (0 to 159, 160 to 319, ...) at most 160 rows name the same one
- expert_weights: float32 [640, 2], P('sp'), may hold values from 0.1 to 1
- gate_proj: bfloat16 [4, 4096, 2048], P('sp', None, 'tp'), may hold values from -0.25 to 0.25
- up_proj: bfloat16 [4, 4096, 2048], P('sp', None, 'tp'), may hold values from -0.25 to 0.25
- down_proj: bfloat16 [4, 2048, 4096], P('sp', 'tp'), may hold values from -0.125 to 0.125
- out_proj: bfloat16 [4096, 4096], P('tp'), may hold values from -0.09375 to 0.09375
- query_rows: bfloat16 [640, 4096], P('sp', 'tp'), may hold values from -6 to 6
- key_rows: bfloat16 [640, 4096], P('sp', 'tp'), may hold values from -6 to 6
- value_rows: bfloat16 [640, 4096], P('sp', 'tp'), may hold values from -6 to 6
- retention_out: bfloat16 [640, 4096], P('sp', 'tp'), may hold values from -6 to 6
- log_decay: float32 [640, 16], P('sp', 'tp'), may hold values from -2 to 0
- entry_state: float32 [4, 16, 256, 256], P('sp', 'tp'), may hold values from -24 to 24
Outputs:
- gate_grad: bfloat16 [4, 4096, 2048], P('sp', None, 'tp')
- up_grad: bfloat16 [4, 4096, 2048], P('sp', None, 'tp')
- down_grad: bfloat16 [4, 2048, 4096], P('sp', 'tp')
- proj_grad: float32 [4096, 4096], P('sp', 'tp')
- query_grad: bfloat16 [640, 4096], P('sp', 'tp')
- key_grad: bfloat16 [640, 4096], P('sp', 'tp')
- value_grad: bfloat16 [640, 4096], P('sp', 'tp')
Inputs may be any that keep to these rules, and one draw needn't show every extreme that they name: `expert_ids`: each row names 2 different experts. Among the rows of one device, no expert is named by more than 160 rows, and in every draw some expert is named by exactly 160 rows of some device.
All inputs are finite; a program needn't handle non-finite values.
Results may differ from a plain program's by a relative error of at most 0.025.
The roundings to bfloat16 on the way count: a program that leaves them out, or rounds other values in their place, can miss the bound.
Values may be sent and summed in bfloat16 or wider, within the bound.
A program may use at most 128 MiB of HBM per device.

v0:
```python
import jax
import jax.numpy as jnp
from jax import lax
from jax.sharding import Mesh, PartitionSpec as P

CLAMP_LIMIT = 7.0
GATE_ALPHA = 1.702
NORM_EPSILON = 1e-05
CORES = 2
SWAP = [(0, 1), (1, 0)]


def activate(gate_pre, up_pre):
    gate_clamped = jnp.minimum(gate_pre, CLAMP_LIMIT)
    up_clamped = jnp.clip(up_pre, -CLAMP_LIMIT, CLAMP_LIMIT)
    return (up_clamped + 1.0) * gate_clamped * jax.nn.sigmoid(GATE_ALPHA * gate_clamped)


def contract_rows(left, right):
    return lax.dot_general(
        left, right, (((0,), (0,)), ((), ())), preferred_element_type=jnp.float32
    )


def contract_cols(left, right):
    return lax.dot_general(
        left, right, (((1,), (1,)), ((), ())), preferred_element_type=jnp.float32
    )


def dots(spec, left, right):
    return jnp.einsum(
        spec,
        left.astype(jnp.bfloat16),
        right.astype(jnp.bfloat16),
        preferred_element_type=jnp.float32,
    )


def local(
    residual_mid,
    out_grad,
    norm_gain,
    expert_ids,
    expert_weights,
    gate_proj,
    up_proj,
    down_proj,
    out_proj,
    query_rows,
    key_rows,
    value_rows,
    retention_out,
    log_decay,
    entry_state,
):
    token_count, width = residual_mid.shape
    segs = lax.axis_size("sp")
    depth = lax.axis_size("z")
    seg = lax.axis_index("sp")
    core = lax.axis_index("core")
    half = token_count // CORES
    share = half // depth

    def rows_of(array, start, count):
        return lax.dynamic_slice_in_dim(array, start, count, axis=0)

    def normalize(rows):
        wide = rows.astype(jnp.float32)
        inverse = lax.rsqrt(jnp.mean(wide * wide, axis=1, keepdims=True) + NORM_EPSILON)
        return wide * inverse, inverse

    grad_own = lax.all_gather(rows_of(out_grad, core * half, half), "sp").reshape(-1, width)
    normed_half = (normalize(rows_of(residual_mid, core * half, half))[0] * norm_gain).astype(
        jnp.bfloat16
    )
    normed_own = lax.all_gather(normed_half, "sp").reshape(-1, width)
    grad_other = lax.ppermute(grad_own, "core", SWAP)
    normed_other = lax.ppermute(normed_own, "core", SWAP)

    experts = jnp.arange(segs, dtype=jnp.int32)
    route = jnp.sum(
        jnp.where(expert_ids.T[None] == experts[:, None, None], expert_weights.T[None], 0.0), axis=1
    )
    heads_here = log_decay.shape[1]
    small = jnp.concatenate([route.reshape(-1), jnp.sum(log_decay, axis=0)])
    smalls = lax.all_gather(small, "sp")
    routes = smalls[:, : segs * token_count].reshape(segs, segs, token_count)
    seg_decay = smalls[:, segs * token_count :]
    here = lax.dynamic_index_in_dim(routes, seg, axis=1, keepdims=False)
    here = here.reshape(segs, CORES, half)
    weight_own = lax.dynamic_index_in_dim(here, core, axis=1, keepdims=False).reshape(-1, 1)
    weight_other = lax.dynamic_index_in_dim(here, 1 - core, axis=1, keepdims=False).reshape(-1, 1)

    gate_weight = gate_proj[0]
    up_weight = up_proj[0]
    down_weight = down_proj[0]

    def expert(rows_in, rows_out, weight):
        rows_grad = (weight * rows_out.astype(jnp.float32)).astype(jnp.bfloat16)
        gate_pre = jnp.dot(rows_in, gate_weight, preferred_element_type=jnp.float32)
        up_pre = jnp.dot(rows_in, up_weight, preferred_element_type=jnp.float32)
        hidden, pullback = jax.vjp(activate, gate_pre, up_pre)
        gate_back, up_back = pullback(contract_cols(rows_grad, down_weight))
        gate_back = gate_back.astype(jnp.bfloat16)
        up_back = up_back.astype(jnp.bfloat16)
        part = contract_cols(gate_back, gate_weight) + contract_cols(up_back, up_weight)
        return part, rows_grad, hidden.astype(jnp.bfloat16), gate_back, up_back

    part_own, cot_own, hidden_own, gate_back_own, up_back_own = expert(
        normed_own, grad_own, weight_own
    )
    part_other, cot_other, hidden_other, gate_back_other, up_back_other = expert(
        normed_other, grad_other, weight_other
    )
    part_got = lax.ppermute(part_other.astype(jnp.bfloat16), "core", SWAP)
    part_pair = (part_own + part_got.astype(jnp.float32)).astype(jnp.bfloat16)
    part_seg = lax.psum_scatter(
        part_pair.reshape(segs, half, width), "sp", scatter_dimension=0, tiled=False
    )
    mixed_grad = lax.psum_scatter(
        part_seg.reshape(depth, share, width), "z", scatter_dimension=0, tiled=False
    ).astype(jnp.float32)

    down_grad = (contract_rows(hidden_own, cot_own) + contract_rows(hidden_other, cot_other)).astype(
        jnp.bfloat16
    )[None]
    gate_grad = (
        contract_rows(normed_own, gate_back_own) + contract_rows(normed_other, gate_back_other)
    ).astype(jnp.bfloat16)[None]
    up_grad = (
        contract_rows(normed_own, up_back_own) + contract_rows(normed_other, up_back_other)
    ).astype(jnp.bfloat16)[None]

    start = core * half + lax.axis_index("z") * share
    scaled, inverse = normalize(rows_of(residual_mid, start, share))
    weighted = norm_gain * mixed_grad
    inner = jnp.mean(scaled * weighted, axis=1, keepdims=True)
    resid_part = (
        rows_of(out_grad, start, share).astype(jnp.float32)
        + inverse * (weighted - scaled * inner)
    ).astype(jnp.bfloat16)
    resid_grad = lax.all_gather(resid_part, ("core", "z"), axis=0, tiled=False).reshape(
        token_count, width
    )
    columns = lax.all_to_all(
        resid_part.reshape(share, segs, width // segs).transpose(1, 0, 2),
        "sp",
        split_axis=0,
        concat_axis=0,
        tiled=True,
    )
    columns = lax.all_gather(columns, ("core", "z"), axis=0, tiled=False).reshape(
        segs * token_count, -1
    )
    outs = lax.all_gather(retention_out, "sp")
    outs = outs.reshape(segs, CORES * depth, share, -1).transpose(1, 0, 2, 3)
    outs = outs.reshape(segs * token_count, -1)
    proj_grad = contract_rows(columns, outs)

    head_grad = contract_cols(resid_grad, out_proj).astype(jnp.bfloat16)

    def split_heads(rows):
        return rows.reshape(token_count, heads_here, -1).transpose(1, 0, 2)

    queries = split_heads(query_rows)
    key_heads = split_heads(key_rows)
    value_heads = split_heads(value_rows)
    grad_heads = split_heads(head_grad)
    key_scale = queries.shape[2] ** (-0.5)
    running = jnp.cumsum(log_decay, axis=0).T
    from_start = jnp.exp(running)
    to_end = jnp.exp(running[:, -1:] - running)
    position = jnp.arange(token_count, dtype=jnp.int32)
    causal = (position[:, None] >= position[None, :])[None]
    spread = jnp.where(causal, running[:, :, None] - running[:, None, :], 0.0)
    weights = jnp.where(causal, jnp.exp(spread), 0.0)
    local_state = dots("htk,hte->hke", from_start[:, :, None] * queries, grad_heads)
    states = lax.all_gather(local_state.astype(jnp.bfloat16), "sp")
    order = jnp.arange(segs, dtype=jnp.int32)
    between = (order[None, :] > seg) & (order[None, :] < order[:, None])
    passed = jnp.exp(jnp.sum(jnp.where(between[:, :, None], seg_decay[None], 0.0), axis=1))
    passed = jnp.where(order[:, None] > seg, passed, 0.0)
    later_state = jnp.sum(passed[:, :, None, None] * states.astype(jnp.float32), axis=0)
    entry = entry_state[0]
    grad_scores = dots("hte,hse->hts", grad_heads, value_heads) * weights
    key_scores = dots("htk,hsk->hts", queries, key_heads) * weights
    query_grad = key_scale * (
        dots("hts,hsk->htk", grad_scores, key_heads)
        + from_start[:, :, None] * dots("hte,hke->htk", grad_heads, entry)
    )
    key_grad = key_scale * (
        dots("hts,htk->hsk", grad_scores, queries)
        + to_end[:, :, None] * dots("hse,hke->hsk", value_heads, later_state)
    )
    value_grad = key_scale * (
        dots("hts,hte->hse", key_scores, grad_heads)
        + to_end[:, :, None] * dots("hsk,hke->hse", key_heads, later_state)
    )

    def merge_heads(heads_rows):
        return heads_rows.transpose(1, 0, 2).reshape(token_count, -1).astype(jnp.bfloat16)

    return (
        gate_grad,
        up_grad,
        down_grad,
        proj_grad,
        merge_heads(query_grad),
        merge_heads(key_grad),
        merge_heads(value_grad),
    )


def solution(mesh):
    segs, split = mesh.shape["sp"], mesh.shape["tp"]
    fine = Mesh(mesh.devices.reshape(segs, split // CORES, CORES), ("sp", "z", "core"))
    tp = ("z", "core")
    placed = (
        P("sp", None),
        P("sp", None),
        P(),
        P("sp", None),
        P("sp", None),
        P("sp", None, tp),
        P("sp", None, tp),
        P("sp", tp, None),
        P(tp, None),
        P("sp", tp),
        P("sp", tp),
        P("sp", tp),
        P("sp", tp),
        P("sp", tp),
        P("sp", tp, None, None),
    )
    return jax.shard_map(
        local,
        mesh=fine,
        in_specs=placed,
        out_specs=(
            P("sp", None, tp),
            P("sp", None, tp),
            P("sp", tp, None),
            P("sp", tp),
            P("sp", tp),
            P("sp", tp),
            P("sp", tp),
        ),
        check_vma=False,
    )
```

profile of v0, /device:TPU:27, one launch (start us, length us, event | category | flops | bytes accessed | tf_op | source)
XLA Modules:
  0.0 292.3 jit_solution(13660346596878332138)
XLA Ops:
  7.3 1.5 fusion.30
  8.8 2.2 fusion.32
  11.0 0.9 constant_dynamic-slice_fusion
  12.0 39.4 %all-gather.14.cloned.1.call-done = bf16[320,4096]{1,0:T(8,128)(2,1)} async-done(((bf16[80,4096]{1,0:T(8,128)(2,1)}), bf16[320,4096]{1,0:T(8,128)(2,1)}) %all-gather.14.cloned.1.call-update) | async-done | bytes 2621456 | tf_op jit(solution)/shard_map/all_gather | solution.py:77
  51.4 0.8 collective-permute-start
  52.3 41.1 %all-gather.16.cloned.1.call-done = bf16[320,4096]{1,0:T(8,128)(2,1)} async-done(((bf16[80,4096]{1,0:T(8,128)(2,1)}), bf16[320,4096]{1,0:T(8,128)(2,1)}) %all-gather.16.cloned.1.call-update) | async-done | bytes 2621456 | tf_op jit(solution)/shard_map/all_gather | solution.py:73
  93.4 0.8 collective-permute-start.1
  95.8 10.3 %all-reduce.1 = f32[2568]{0:T(1024)S(1)} all-reduce(f32[2568]{0:T(1024)S(1)} %maximum_dynamic-update-slice_fusion), channel_id=3, replica_groups=mesh['sp'=4,'z'=4,'core'=2] {'sp'}, use_global_device_ids=true, to_apply=%add.1 | all-reduce | flops 2568 | bytes 20544
  107.6 3.2 %fusion.18 = f32[320,256]{1,0:T(8,128)S(1)} fusion(bf16[320,4096]{1,0:T(8,128)(2,1)} %collective-permute-done, bf16[1,4096,256]{2,1,0:T(8,128)(2,1)} %param.23), kind=kOutput, calls=%fused_computation.28 | convolution fusion | flops 671088640 | bytes 5046272 | tf_op jit(solution)/shard_map/dot_general | solution.py:101
  110.9 2.7 fusion.24
  113.7 3.2 %fusion.72 = (bf16[320,256]{1,0:T(8,128)(2,1)S(1)}, bf16[320,256]{1,0:T(8,128)(2,1)S(1)}) fusion(f32[320,256]{1,0:T(8,128)S(1)} %fusion.24, f32[320,256]{1,0:T(8,128)S(1)} %fusion.18, bf16[1,256,4096]{2,1,0:T(8,128)(2,1)S(1)} %copy-done.26, bf16[320,4096]{1,0:T(8,128)(2,1)} %collective-permute-done.1, f32[320]{0:T(512)S(1)} %mul.248), kind=kOutput, calls=%fused_computation.99 | convolution fusion | flops 677888000 | bytes 5702912 | tf_op jit(solution)/shard_map/dot_general | solution.py:26
  116.9 0.9 fusion.14
  117.8 1.0 fusion
  118.8 3.8 %collective-permute-start.2 = (bf16[320,4096]{1,0:T(8,128)(2,1)S(1)}, bf16[320,4096]{1,0:T(8,128)(2,1)S(1)}, u32[]{:S(2)}, u32[]{:S(2)}) collective-permute-start(bf16[320,4096]{1,0:T(8,128)(2,1)S(1)} %fusion), channel_id=1, source_target_pairs={{0,1},{1,0},{2,3},{3,2},{4,5},{5,4},{6,7},{7,6},{8,9},{9,8},{10,11... | collective-permute-start | bytes 7864328 | tf_op jit(solution)/shard_map/ppermute | solution.py:116
  122.6 0.8 multiply_convert_fusion.2
  123.5 1.0 fusion.12
  124.5 0.7 copy-done.3
  125.2 0.9 fusion.20
  126.1 1.9 fusion.74
  127.9 0.9 fusion.16
  128.8 2.6 add_convert_fusion
  131.5 40.5 %reduce-scatter.7.cloned.1.call-done = bf16[1,80,4096]{2,1,0:T(8,128)(2,1)} async-done(((bf16[4,80,4096]{2,1,0:T(8,128)(2,1)}), bf16[1,80,4096]{2,1,0:T(8,128)(2,1)}) %reduce-scatter.7.cloned.1.call-update) | async-done | bytes 655376
  172.1 2.1 reshape_reduce_scatter.3
  175.4 1.1 fusion.60
  176.5 18.9 %reduce-scatter.5.cloned.1.call-done = bf16[1,20,4096]{2,1,0:T(8,128)(2,1)} async-done(((bf16[4,20,4096]{2,1,0:T(8,128)(2,1)}), bf16[1,20,4096]{2,1,0:T(8,128)(2,1)}) %reduce-scatter.5.cloned.1.call-update) | async-done | bytes 163856 | tf_op jit(solution)/shard_map/reduce_scatter | solution.py:121
  195.5 1.3 fusion.55
  196.7 2.0 fusion.59
  199.0 9.0 %all-gather.4 = bf16[640,512]{1,0:T(8,128)(2,1)S(1)} all-gather(bf16[160,512]{1,0:T(8,128)(2,1)S(1)} %copy-done.21), channel_id=6, replica_groups=mesh['sp'=4,'z'=4,'core'=2] {'sp'}, dimensions={0}, use_global_device_ids=true | all-gather | bytes 819200 | tf_op jit(solution)/shard_map/all_gather | solution.py:156
  208.5 5.3 %fusion.7 = f32[256,4096]{1,0:T(8,128)} fusion(f32[320]{0:T(512)S(1)} %mul.266, bf16[320,4096]{1,0:T(8,128)(2,1)} %all-gather.16.cloned.1.call-done, f32[320,256]{1,0:T(8,128)S(1)} %copy-done.13, f32[320,256]{1,0:T(8,128)S(1)} %copy-done.14), kind=kOutput, calls=%fused_computation.16 | convolution fusion | flops 675840000 | bytes 7472384 | tf_op jit(solution)/shard_map/dot_general | solution.py:20
  213.9 0.7 copy.198
  214.6 4.1 %all-to-all-start = ((bf16[4,20,1024]{2,1,0:T(8,128)(2,1)}), bf16[4,20,1024]{2,1,0:T(8,128)(2,1)S(1)}, u32[]{:S(2)}, u32[]{:S(2)}) async-start(bf16[4,20,1024]{2,1,0:T(8,128)(2,1)} %bitcast.202), calls=%async_computation.1 | async-start | bytes 393216 | tf_op jit(solution)/shard_map/all_to_all | solution.py:146
  218.8 5.0 %fusion.119 = f32[4096,256]{1,0:T(8,128)} fusion(bf16[320,4096]{1,0:T(8,128)(2,1)} %all-gather.14.cloned.1.call-done, bf16[320,256]{1,0:T(8,128)(2,1)S(1)} %get-tuple-element.23), kind=kOutput, calls=%fused_computation.180 | convolution fusion | flops 671088640 | bytes 6979584 | tf_op jit(solution)/shard_map/dot_general | solution.py:20
  223.8 0.7 copy-done.8
  224.6 3.2 %fusion.118 = f32[4096,256]{1,0:T(8,128)S(1)} fusion(bf16[320,4096]{1,0:T(8,128)(2,1)} %all-gather.14.cloned.1.call-done, bf16[320,256]{1,0:T(8,128)(2,1)S(1)} %get-tuple-element.24), kind=kOutput, calls=%fused_computation.179 | convolution fusion | flops 671088640 | bytes 6979584 | tf_op jit(solution)/shard_map/dot_general | solution.py:20
  227.8 4.4 %fusion.5 = bf16[1,4096,256]{2,1,0:T(8,128)(2,1)} fusion(f32[4096,256]{1,0:T(8,128)S(1)} %copy-done.2, bf16[320,4096]{1,0:T(8,128)(2,1)} %collective-permute-done, bf16[320,256]{1,0:T(8,128)(2,1)S(1)} %get-tuple-element.21), kind=kOutput, calls=%fused_computation.14 | convolution fusion | flops 673185792 | bytes 9076736 | tf_op jit(solution)/shard_map/dot_general | solution.py:20
  232.2 4.6 %fusion.6 = bf16[1,4096,256]{2,1,0:T(8,128)(2,1)} fusion(f32[4096,256]{1,0:T(8,128)S(1)} %fusion.118, bf16[320,4096]{1,0:T(8,128)(2,1)} %collective-permute-done, bf16[320,256]{1,0:T(8,128)(2,1)S(1)} %get-tuple-element.22), kind=kOutput, calls=%fused_computation.15 | convolution fusion | flops 673185792 | bytes 9076736 | tf_op jit(solution)/shard_map/dot_general | solution.py:20
  236.7 4.6 %fusion.4 = bf16[1,256,4096]{2,1,0:T(8,128)(2,1)} fusion(f32[256,4096]{1,0:T(8,128)S(1)} %copy-done.4, bf16[320,4096]{1,0:T(8,128)(2,1)} %collective-permute-done.1, f32[320]{0:T(512)S(1)} %mul.248, f32[320,256]{1,0:T(8,128)S(1)} %copy-done.16, f32[320,256]{1,0:T(8,128)S(1)} %copy-done.18), kind=kOutput, calls=%fused_computation.13 | convolution fusion | flops 677937152 | bytes 9569536 | tf_op jit(solution)/shard_map/dot_general | solution.py:20
  241.3 1.5 reshape.213
  242.9 3.8 %convolution_convert_fusion.1 = bf16[160,512]{1,0:T(8,128)(2,1)S(1)} fusion(bf16[160,4096]{1,0:T(8,128)(2,1)S(1)} %reshape.213, bf16[512,4096]{1,0:T(8,128)(2,1)} %param.26), kind=kOutput, calls=%fused_computation.65 | convolution fusion | flops 671170560 | bytes 5668864 | tf_op jit(solution)/shard_map/dot_general | solution.py:26
  247.0 1.0 convolution_convert_fusion
  248.5 0.7 copy.138
  249.5 1.2 convolution_bitcast_fusion.4
  250.7 1.8 all-gather.18.cloned.1.call-done
  252.4 3.9 %convolution_bitcast_fusion = f32[1024,512]{1,0:T(8,128)} fusion(bf16[8,4,20,1024]{3,2,1,0:T(8,128)(2,1)} %bitcast.234, bf16[4,8,20,512]{3,2,1,0:T(8,128)(2,1)S(1)} %reshape.187), kind=kOutput, calls=%fused_computation.40 | convolution fusion | flops 671088640 | bytes 4063232 | tf_op jit(solution)/shard_map/dot_general | solution.py:20
  256.3 24.8 %all-gather.20.cloned.1.call-done = bf16[8,256,256]{2,1,0:T(8,128)(2,1)} async-done(((bf16[2,256,256]{2,1,0:T(8,128)(2,1)}), bf16[8,256,256]{2,1,0:T(8,128)(2,1)}) %all-gather.20.cloned.1.call-update) | async-done | bytes 1048592 | tf_op jit(solution)/shard_map/all_gather | solution.py:179
  281.1 1.5 fusion.9
  282.7 1.2 fusion.50
  283.8 0.7 copy.140
  (118 shorter events, 6.8 us)
Async XLA Ops:
  7.2 103.7 %copy-start = (bf16[1,4096,256]{2,1,0:T(8,128)(2,1)S(1)}, bf16[1,4096,256]{2,1,0:T(8,128)(2,1)}, u32[]{:S(2)}) copy-start(bf16[1,4096,256]{2,1,0:T(8,128)(2,1)} %param.24) | copy-start | bytes 6291460
  7.2 87.1 %copy-start.27 = (u32[32]{0:T(128)S(1)}, u32[32]{0:T(128)}, u32[]{:S(2)}) copy-start(u32[32]{0:T(128)} %constant.80) | copy-start | bytes 388
  7.2 3.8 %copy-start.10 = (bf16[160,4096]{1,0:T(8,128)(2,1)S(1)}, bf16[160,4096]{1,0:T(8,128)(2,1)}, u32[]{:S(2)}) copy-start(bf16[160,4096]{1,0:T(8,128)(2,1)} %param.19) | copy-start | bytes 3932164
  7.2 87.0 %copy-start.24 = (f32[160,2]{0,1:T(2,128)S(1)}, f32[160,2]{0,1:T(2,128)}, u32[]{:S(2)}) copy-start(f32[160,2]{0,1:T(2,128)} %param.22) | copy-start | bytes 3844
  7.2 87.0 %copy-start.25 = (s32[160,2]{0,1:T(2,128)S(1)}, s32[160,2]{0,1:T(2,128)}, u32[]{:S(2)}) copy-start(s32[160,2]{0,1:T(2,128)} %param.21) | copy-start | bytes 3844
  7.2 88.3 %copy-start.23 = (f32[160,2]{0,1:T(2,128)S(1)}, f32[160,2]{0,1:T(2,128)}, u32[]{:S(2)}) copy-start(f32[160,2]{0,1:T(2,128)} %param.31) | copy-start | bytes 3844
  7.2 44.2 %all-gather.14.cloned.1.call-start = ((), (), s32[]{:S(2)}) async-start(), calls=%async_computation.4 | async-start | bytes 3276800 | tf_op jit(solution)/shard_map/all_gather | solution.py:77
  11.0 82.4 %all-gather.16.cloned.1.call-start = ((), (), s32[]{:S(2)}) async-start(), calls=%async_computation.5 | async-start | bytes 3276800 | tf_op jit(solution)/shard_map/all_gather | solution.py:73
  12.0 160.1 %reduce-scatter.7.cloned.1.call-start = ((), (), s32[]{:S(2)}) async-start(), calls=%async_computation.9 | async-start | bytes 3276800
  51.4 56.2 %collective-permute-start = (bf16[320,4096]{1,0:T(8,128)(2,1)}, bf16[320,4096]{1,0:T(8,128)(2,1)}, u32[]{:S(2)}, u32[]{:S(2)}) collective-permute-start(bf16[320,4096]{1,0:T(8,128)(2,1)} %all-gather.14.cloned.1.call-done), channel_id=1, source_target_pairs={{0,1},{1,0},{2,3},{3,2},{4,5},{5,4},{6,7},{7,6},{8,9},{9,8},{10,11... | collective-permute-start | bytes 7864328 | tf_op jit(solution)/shard_map/ppermute | solution.py:79
  93.4 20.3 %collective-permute-start.1 = (bf16[320,4096]{1,0:T(8,128)(2,1)}, bf16[320,4096]{1,0:T(8,128)(2,1)}, u32[]{:S(2)}, u32[]{:S(2)}) collective-permute-start(bf16[320,4096]{1,0:T(8,128)(2,1)} %all-gather.16.cloned.1.call-done), channel_id=1, source_target_pairs={{0,1},{1,0},{2,3},{3,2},{4,5},{5,4},{6,7},{7,6},{8,9},{9,8},{10,11... | collective-permute-start | bytes 7864328 | tf_op jit(solution)/shard_map/ppermute | solution.py:78
  110.9 2.8 copy-start.15
  110.9 2.8 copy-start.26
  113.7 3.3 %copy-start.17 = (f32[320,256]{1,0:T(8,128)}, f32[320,256]{1,0:T(8,128)S(1)}, u32[]{:S(2)}) copy-start(f32[320,256]{1,0:T(8,128)S(1)} %fusion.24) | copy-start | bytes 983044
  113.7 3.3 %copy-start.6 = (bf16[1,4096,256]{2,1,0:T(8,128)(2,1)S(1)}, bf16[1,4096,256]{2,1,0:T(8,128)(2,1)}, u32[]{:S(2)}) copy-start(bf16[1,4096,256]{2,1,0:T(8,128)(2,1)} %param.23) | copy-start | bytes 6291460
  117.8 4.8 %copy-start.5 = (bf16[320,4096]{1,0:T(8,128)(2,1)S(1)}, bf16[320,4096]{1,0:T(8,128)(2,1)}, u32[]{:S(2)}) copy-start(bf16[320,4096]{1,0:T(8,128)(2,1)} %all-gather.16.cloned.1.call-done) | copy-start | bytes 7864324
  118.8 10.0 %collective-permute-start.2 = (bf16[320,4096]{1,0:T(8,128)(2,1)S(1)}, bf16[320,4096]{1,0:T(8,128)(2,1)S(1)}, u32[]{:S(2)}, u32[]{:S(2)}) collective-permute-start(bf16[320,4096]{1,0:T(8,128)(2,1)S(1)} %fusion), channel_id=1, source_target_pairs={{0,1},{1,0},{2,3},{3,2},{4,5},{5,4},{6,7},{7,6},{8,9},{9,8},{10,11... | collective-permute-start | bytes 7864328 | tf_op jit(solution)/shard_map/ppermute | solution.py:116
  123.5 1.7 copy-start.3
  126.1 1.9 copy-start.12
  131.5 64.0 %copy-start.22 = (f32[4096]{0:T(1024)S(1)}, f32[4096]{0:T(1024)}, u32[]{:S(2)}) copy-start(f32[4096]{0:T(1024)} %param.20) | copy-start | bytes 49156
  131.5 67.6 %copy-start.21 = (bf16[160,512]{1,0:T(8,128)(2,1)S(1)}, bf16[160,512]{1,0:T(8,128)(2,1)}, u32[]{:S(2)}) copy-start(bf16[160,512]{1,0:T(8,128)(2,1)} %param.30) | copy-start | bytes 491524
  131.5 64.0 %reduce-scatter.5.cloned.1.call-start = ((), (), s32[]{:S(2)}) async-start(), calls=%async_computation.3 | async-start | bytes 983040 | tf_op jit(solution)/shard_map/reduce_scatter | solution.py:121
  174.2 34.3 %copy-start.13 = (f32[320,256]{1,0:T(8,128)S(1)}, f32[320,256]{1,0:T(8,128)}, u32[]{:S(2)}) copy-start(f32[320,256]{1,0:T(8,128)} %copy-done.12) | copy-start | bytes 983044
  174.2 34.3 %copy-start.14 = (f32[320,256]{1,0:T(8,128)S(1)}, f32[320,256]{1,0:T(8,128)}, u32[]{:S(2)}) copy-start(f32[320,256]{1,0:T(8,128)} %get-tuple-element.28) | copy-start | bytes 983044
  174.2 67.2 %all-gather.22.cloned.1.call-start = ((), (), s32[]{:S(2)}) async-start(), calls=%async_computation.8 | async-start | bytes 1769472 | tf_op jit(solution)/shard_map/all_gather | solution.py:143
  208.5 5.3 %copy-start.7 = (bf16[20,4096]{1,0:T(8,128)(2,1)S(1)}, bf16[20,4096]{1,0:T(8,128)(2,1)}, u32[]{:S(2)}) copy-start(bf16[20,4096]{1,0:T(8,128)(2,1)} %fusion.59) | copy-start | bytes 491524
  214.6 9.2 %all-to-all-start = ((bf16[4,20,1024]{2,1,0:T(8,128)(2,1)}), bf16[4,20,1024]{2,1,0:T(8,128)(2,1)S(1)}, u32[]{:S(2)}, u32[]{:S(2)}) async-start(bf16[4,20,1024]{2,1,0:T(8,128)(2,1)} %bitcast.202), calls=%async_computation.1 | async-start | bytes 393216 | tf_op jit(solution)/shard_map/all_to_all | solution.py:146
  218.7 33.7 %all-gather.18.cloned.1.call-start = ((), (), s32[]{:S(2)}) async-start(), calls=%async_computation.6 | async-start | bytes 1769472 | tf_op jit(solution)/shard_map/all_gather | solution.py:153
  223.8 0.7 copy-start.8
  224.5 56.6 %all-gather.20.cloned.1.call-start = ((), (), s32[]{:S(2)}) async-start(), calls=%async_computation.7 | async-start | bytes 1310720 | tf_op jit(solution)/shard_map/all_gather | solution.py:179
  224.5 3.2 %copy-start.2 = (f32[4096,256]{1,0:T(8,128)S(1)}, f32[4096,256]{1,0:T(8,128)}, u32[]{:S(2)}) copy-start(f32[4096,256]{1,0:T(8,128)} %fusion.119) | copy-start | bytes 12582916
  232.2 4.6 %copy-start.4 = (f32[256,4096]{1,0:T(8,128)S(1)}, f32[256,4096]{1,0:T(8,128)}, u32[]{:S(2)}) copy-start(f32[256,4096]{1,0:T(8,128)} %fusion.7) | copy-start | bytes 12582916
  232.2 4.6 %copy-start.16 = (f32[320,256]{1,0:T(8,128)S(1)}, f32[320,256]{1,0:T(8,128)}, u32[]{:S(2)}) copy-start(f32[320,256]{1,0:T(8,128)} %copy-done.15) | copy-start | bytes 983044
  232.2 4.6 %copy-start.18 = (f32[320,256]{1,0:T(8,128)S(1)}, f32[320,256]{1,0:T(8,128)}, u32[]{:S(2)}) copy-start(f32[320,256]{1,0:T(8,128)} %copy-done.17) | copy-start | bytes 983044
  242.9 3.9 %copy-start.20 = (bf16[160,512]{1,0:T(8,128)(2,1)S(1)}, bf16[160,512]{1,0:T(8,128)(2,1)}, u32[]{:S(2)}) copy-start(bf16[160,512]{1,0:T(8,128)(2,1)} %param.29) | copy-start | bytes 491524
  242.9 4.1 %copy-start.19 = (bf16[160,512]{1,0:T(8,128)(2,1)S(1)}, bf16[160,512]{1,0:T(8,128)(2,1)}, u32[]{:S(2)}) copy-start(bf16[160,512]{1,0:T(8,128)(2,1)} %param.27) | copy-start | bytes 491524
  242.9 5.2 %copy-start.9 = (bf16[160,512]{1,0:T(8,128)(2,1)S(1)}, bf16[160,512]{1,0:T(8,128)(2,1)}, u32[]{:S(2)}) copy-start(bf16[160,512]{1,0:T(8,128)(2,1)} %param.28) | copy-start | bytes 491524
  246.8 1.5 copy-start.11
  252.4 33.0 %copy-start.1 = (bf16[1,4096,256]{2,1,0:T(8,128)(2,1)S(1)}, bf16[1,4096,256]{2,1,0:T(8,128)(2,1)}, u32[]{:S(2)}) copy-start(bf16[1,4096,256]{2,1,0:T(8,128)(2,1)} %param.24) | copy-start | bytes 6291460
Sparse Core Ops, SparseCore 0:
  11.1 40.2 all-gather.13
  53.8 39.4 all-gather.15
  131.6 40.3 reduce-scatter.6
  174.8 20.6 reduce-scatter.4
  198.9 26.0 all-gather.21
  226.4 25.9 all-gather.17
  254.3 26.8 all-gather.19
where the time goes:
time: 295 us; the launch traced here: 292 us
  waiting for transfers between devices  167 us (57%)
  matrix products  57.6 us (20%)
  blocking collectives  19.3 us (7%)
  between operations  15.3 us (5%)
  local copies, waits for them, and re-layouts  11.9 us (4%)
  other arithmetic  11.7 us (4%)
  starting transfers between devices  9.89 us (3%)
    all_gather x1, waiting for transfers between devices, local(): lax.all_gather(rows_of(out_grad, core * half, half), 'sp')  41.1 us
    unnamed x8, waiting for transfers between devices  40.6 us
    all_gather x1, waiting for transfers between devices, local(): normed_own = lax.all_gather(normed_half, 'sp').reshape(-1, width)  39.4 us
    dot_general x7, matrix products, contract_rows(): lax.dot_general(left, right, (((0,), (0,)), ((), ())), preferred_element_...  30.9 us
    all_gather x1, waiting for transfers between devices, local(): states = lax.all_gather(local_state.astype(jnp.bfloat16), 'sp')  24.8 us
    reduce_scatter x1, waiting for transfers between devices, local(): lax.psum_scatter(part_seg.reshape(depth, share, width), 'z', scatter_dime...  18.9 us
    dot_general x7, matrix products, contract_cols(): lax.dot_general(left, right, (((1,), (1,)), ((), ())), preferred_element_...  13.4 us
    unnamed x1, blocking collectives  10.3 us
  transfers between devices with their start and end apart: 11, of which 6 were waited for; matrix products, arithmetic and copies ran while one was open for 20% of the time, Pallas kernels for 0%

commit v1 on v0

--- a/solution.py
+++ b/solution.py
@@ -1,6 +1,10 @@
+import functools
+
 import jax
 import jax.numpy as jnp
 from jax import lax
+from jax.experimental import pallas as pl
+from jax.experimental.pallas import tpu as pltpu
 from jax.sharding import Mesh, PartitionSpec as P
 
 CLAMP_LIMIT = 7.0
@@ -37,7 +41,7 @@
     )
 
 
-def local(
+def local_general(
     residual_mid,
     out_grad,
     norm_gain,
@@ -212,6 +216,580 @@
     )
 
 
+ROWS = 16
+MESH_ID = pl.DeviceIdType.MESH
+
+
+def square_kernel(
+    raw_r_hbm,
+    raw_o_hbm,
+    route_ref,
+    gain_ref,
+    wg_hbm,
+    wu_hbm,
+    wd_hbm,
+    op_hbm,
+    outs_hbm,
+    fq_hbm,
+    ends_ref,
+    gate_out,
+    up_out,
+    down_out,
+    col_out,
+    hg_out,
+    outs_out,
+    fq_out,
+    ends_out,
+    raw_r,
+    raw_o,
+    rin,
+    og,
+    stg,
+    wg,
+    wu,
+    wd,
+    op,
+    part,
+    pin,
+    hid,
+    back,
+    rx,
+    ry,
+    rz1,
+    sd,
+    rd,
+    rz2,
+    wz,
+    inv,
+    msend,
+    mz,
+    rg,
+    col,
+    hga,
+    outs_all,
+    fq_all,
+    ends_all,
+    gout,
+    uout,
+    dout,
+    send_sems,
+    recv_sems,
+    load_sems,
+    store_sems,
+):
+    segs, count, width = rin.shape
+    half = count // CORES
+    depth = segs
+    quarter = width // depth
+    feats = wg.shape[1]
+    g = lax.axis_index("sp")
+    z = lax.axis_index("z")
+    c = lax.axis_index("core")
+    gy_, gx_ = g // 2, g % 2
+    gx = gy_ * 2 + (1 - gx_)
+    gy = (1 - gy_) * 2 + gx_
+    gd = (1 - gy_) * 2 + (1 - gx_)
+    ups = [(z + i) % depth for i in range(1, depth)]
+    downs = [(z + depth - i) % depth for i in range(1, depth)]
+    mine = pl.ds(pl.multiple_of(c * half, ROWS), half)
+    theirs = pl.ds(pl.multiple_of((1 - c) * half, ROWS), half)
+
+    def span(index):
+        return pl.ds(pl.multiple_of(index * quarter, 128), quarter)
+
+    def dev(sp, zz, cc):
+        return {"sp": sp, "z": zz, "core": cc}
+
+    sends = []
+    used = [0]
+
+    def remote(src, dst, target):
+        k = used[0]
+        used[0] += 1
+        copy = pltpu.make_async_remote_copy(
+            src_ref=src,
+            dst_ref=dst,
+            send_sem=send_sems.at[k],
+            recv_sem=recv_sems.at[k],
+            device_id=target,
+            device_id_type=MESH_ID,
+        )
+        sends.append(copy)
+        return copy
+
+    def put(src, dst, target):
+        copy = remote(src, dst, target)
+        copy.start()
+        return copy
+
+    loads = []
+
+    def load(src, dst):
+        copy = pltpu.make_async_copy(src, dst, load_sems.at[len(loads)])
+        copy.start()
+        loads.append(copy)
+        return copy
+
+    stores = []
+
+    def store(src, dst):
+        copy = pltpu.make_async_copy(src, dst, store_sems.at[len(stores)])
+        copy.start()
+        stores.append(copy)
+
+    load_o = load(raw_o_hbm, raw_o)
+    load_r = load(raw_r_hbm, raw_r)
+    load_w = [load(wg_hbm, wg), load(wu_hbm, wu), load(wd_hbm, wd)]
+    load_op = load(op_hbm, op)
+    load_outs = load(outs_hbm, outs_all.at[g])
+    load_fq = load(fq_hbm, fq_all.at[g])
+
+    X, Y, Z = dev(gx, z, c), dev(gy, z, c), dev(gd, z, c)
+    across = dev(g, z, 1 - c)
+    along = [dev(g, zz, c) for zz in ups]
+    barrier = pltpu.get_barrier_semaphore()
+    for target in [X, Y, Z, across] + along:
+        pl.semaphore_signal(barrier, inc=1, device_id=target, device_id_type=MESH_ID)
+
+    lanes = lax.broadcasted_iota(jnp.int32, (ROWS, 128), 1)
+
+    def weigh(base, rows, expert, write):
+        def step(i, carry):
+            r = pl.ds(pl.multiple_of(base + i * ROWS, ROWS), ROWS)
+            w = jnp.sum(jnp.where(lanes == expert, route_ref[r, :], 0.0), axis=1, keepdims=True)
+            write(i, r, (w * raw_o[r, :].astype(jnp.float32)).astype(jnp.bfloat16))
+            return carry
+
+        lax.fori_loop(0, rows // ROWS, step, 0)
+
+    def stage(index):
+        def write(i, r, value):
+            stg[index, pl.ds(pl.multiple_of(i * ROWS, ROWS), ROWS), :] = value
+
+        return write
+
+    def own_write(i, r, value):
+        og[g, r, :] = value
+
+    def normalize(base, rows):
+        def step(i, carry):
+            r = pl.ds(pl.multiple_of(base + i * ROWS, ROWS), ROWS)
+            wide = raw_r[r, :].astype(jnp.float32)
+            inverse = lax.rsqrt(jnp.mean(wide * wide, axis=1, keepdims=True) + NORM_EPSILON)
+            inv[r, :] = jnp.broadcast_to(inverse, (ROWS, 128))
+            rin[g, r, :] = (wide * inverse * gain_ref[...]).astype(jnp.bfloat16)
+            return carry
+
+        lax.fori_loop(0, rows // ROWS, step, 0)
+
+    load_o.wait()
+    weigh(c * half, half, gd, stage(2))
+    pl.semaphore_wait(barrier, 4 + len(along))
+    d_o = put(stg.at[2, :, span(z)], og.at[g, mine, span(z)], Z)
+    load_r.wait()
+    normalize(c * half, half)
+    d_n = put(rin.at[g, mine, span(z)], rin.at[g, mine, span(z)], Z)
+    x_n = put(rin.at[g, mine, :], rin.at[g, mine, :], X)
+    y_n = put(rin.at[g, mine, :], rin.at[g, mine, :], Y)
+    weigh(c * half, half, gx, stage(0))
+    x_o = put(stg.at[0], og.at[g, mine, :], X)
+    weigh(c * half, half, gy, stage(1))
+    y_o = put(stg.at[1], og.at[g, mine, :], Y)
+    normalize((1 - c) * half, half)
+    weigh(0, count, g, own_write)
+
+    def spread(buf):
+        block = buf.at[gd, mine, span(z)]
+        return [put(block, block, t) for t in along] + [put(block, block, across)]
+
+    d_o.wait_recv()
+    o_spread = spread(og)
+    d_n.wait_recv()
+    n_spread = spread(rin)
+
+    for copy in load_w:
+        copy.wait()
+
+    def expert(s):
+        gate_pre = jnp.dot(rin[s], wg[...], preferred_element_type=jnp.float32)
+        up_pre = jnp.dot(rin[s], wu[...], preferred_element_type=jnp.float32)
+        hidden, pullback = jax.vjp(activate, gate_pre, up_pre)
+        gate_back, up_back = pullback(contract_cols(og[s], wd[...]))
+        gate_back = gate_back.astype(jnp.bfloat16)
+        up_back = up_back.astype(jnp.bfloat16)
+        hid[s] = hidden.astype(jnp.bfloat16)
+        back[s, :, :feats] = gate_back
+        back[s, :, feats:] = up_back
+
+        def step(n, carry):
+            rows = pl.ds(pl.multiple_of(n * quarter, 128), quarter)
+            piece = contract_cols(back[s, :, :feats], wg[rows, :]) + contract_cols(
+                back[s, :, feats:], wu[rows, :]
+            )
+            part[s, :, rows] = piece.astype(jnp.bfloat16)
+            return carry
+
+        lax.fori_loop(0, depth, step, 0)
+        return put(part.at[s, theirs, :], pin.at[s], across)
+
+    swap_own = expert(g)
+
+    x_n.wait_recv()
+    f = [put(rin.at[gx, mine, :], rin.at[gx, mine, :], across)]
+    y_n.wait_recv()
+    f.append(put(rin.at[gy, mine, :], rin.at[gy, mine, :], across))
+    for i in range(depth - 1):
+        for buf, group in ((og, o_spread), (rin, n_spread)):
+            group[i].wait_recv()
+            block = buf.at[gd, mine, span(downs[i])]
+            f.append(put(block, block, across))
+    x_o.wait_recv()
+    f.append(put(og.at[gx, mine, :], og.at[gx, mine, :], across))
+    y_o.wait_recv()
+    f.append(put(og.at[gy, mine, :], og.at[gy, mine, :], across))
+    o_spread[-1].wait_recv()
+    n_spread[-1].wait_recv()
+    for copy in f:
+        copy.wait_recv()
+
+    def pair(s, swap, extra=()):
+        swap.wait_recv()
+
+        def step(i, carry):
+            r = pl.ds(pl.multiple_of(c * half + i * ROWS, ROWS), ROWS)
+            q = pl.ds(pl.multiple_of(i * ROWS, ROWS), ROWS)
+            total = part[s, r, :].astype(jnp.float32) + pin[s, q, :].astype(jnp.float32)
+            for ref in extra:
+                total = total + ref[q, :].astype(jnp.float32)
+            part[s, r, :] = total.astype(jnp.bfloat16)
+            return carry
+
+        lax.fori_loop(0, half // ROWS, step, 0)
+
+    swap_d = expert(gd)
+    swap_x = expert(gx)
+    pair(gd, swap_d)
+    d_z = [put(part.at[gd, mine, span(ups[i])], rz1.at[i], along[i]) for i in range(depth - 1)]
+    swap_y = expert(gy)
+    pair(gx, swap_x)
+    x_p = put(part.at[gx, mine, :], rx, X)
+    pair(gy, swap_y)
+    y_p = put(part.at[gy, mine, :], ry, Y)
+
+    def weight_step(n, carry):
+        cols = pl.ds(pl.multiple_of(n * 512, 128), 512)
+        block = contract_rows(rin[:, :, cols].reshape(segs * count, 512), back[...].reshape(segs * count, 2 * feats))
+        gout[cols, :] = block[:, :feats].astype(jnp.bfloat16)
+        uout[cols, :] = block[:, feats:].astype(jnp.bfloat16)
+        return carry
+
+    lax.fori_loop(0, width // 512, weight_step, 0)
+    store(gout, gate_out)
+    store(uout, up_out)
+
+    def z_sum(own, landed, write, more=None):
+        for copy in landed[0]:
+            copy.wait_recv()
+
+        def step(i, carry):
+            q = pl.ds(pl.multiple_of(i * ROWS, ROWS), ROWS)
+            r = pl.ds(pl.multiple_of(c * half + i * ROWS, ROWS), ROWS)
+            total = part[own, r, span(z)].astype(jnp.float32)
+            for k in range(depth - 1):
+                total = total + landed[1][k, q, :].astype(jnp.float32)
+            if more is not None:
+                total = total + more[q, :].astype(jnp.float32)
+            write(q, r, total)
+            return carry
+
+        lax.fori_loop(0, half // ROWS, step, 0)
+
+    def write_sd(q, r, total):
+        sd[q, :] = total.astype(jnp.bfloat16)
+
+    z_sum(gd, (d_z, rz1), write_sd)
+    d_p = put(sd, rd, Z)
+
+    load_outs.wait()
+    load_fq.wait()
+    extras = []
+    for target in (X, Y, Z):
+        extras.append(put(fq_all.at[g], fq_all.at[g], target))
+        extras.append(put(ends_ref, ends_all.at[g], target))
+        extras.append(put(outs_all.at[g], outs_all.at[g], target))
+    ends_all[g] = ends_ref[...]
+
+    x_p.wait_recv()
+    y_p.wait_recv()
+    pair(g, swap_own, (rx, ry))
+    own_z = [put(part.at[g, mine, span(ups[i])], rz2.at[i], along[i]) for i in range(depth - 1)]
+
+    def down_step(n, carry):
+        cols = pl.ds(pl.multiple_of(n * 512, 128), 512)
+        block = contract_rows(
+            hid[...].reshape(segs * count, feats), og[:, :, cols].reshape(segs * count, 512)
+        )
+        dout[:, cols] = block.astype(jnp.bfloat16)
+        return carry
+
+    lax.fori_loop(0, width // 512, down_step, 0)
+    store(dout, down_out)
+
+    d_p.wait_recv()
+
+    def write_m(q, r, total):
+        weighted = gain_ref[:, span(z)] * total
+        scaled = raw_r[r, span(z)].astype(jnp.float32) * inv[r, 0:1]
+        inner = jnp.sum(scaled * weighted, axis=1, keepdims=True)
+        msend[q, :] = jnp.broadcast_to(inner, (ROWS, 128))
+        wz[q, :] = weighted
+
+    z_sum(g, (own_z, rz2), write_m, rd)
+    m_z = [put(msend, mz.at[i], along[i]) for i in range(depth - 1)]
+    for copy in m_z:
+        copy.wait_recv()
+
+    def resid_step(i, carry):
+        q = pl.ds(pl.multiple_of(i * ROWS, ROWS), ROWS)
+        r = pl.ds(pl.multiple_of(c * half + i * ROWS, ROWS), ROWS)
+        inverse = inv[r, 0:1]
+        scaled = raw_r[r, span(z)].astype(jnp.float32) * inverse
+        inner = msend[q, 0:1]
+        for k in range(depth - 1):
+            inner = inner + mz[k, q, 0:1]
+        inner = inner / width
+        grad = raw_o[r, span(z)].astype(jnp.float32) + inverse * (wz[q, :] - scaled * inner)
+        rg[r, span(z)] = grad.astype(jnp.bfloat16)
+        return carry
+
+    lax.fori_loop(0, half // ROWS, resid_step, 0)
+    block = rg.at[mine, span(z)]
+    g_z = [put(block, block, t) for t in along]
+    g_f = [put(block, block, across)]
+    col_copies = [
+        (t, remote(rg.at[mine, span(t)], col.at[g, mine, :], target))
+        for t, target in ((gx, X), (gy, Y), (gd, Z))
+    ]
+
+    def send_columns(q):
+        for t, copy in col_copies:
+
+            @pl.when(q == t)
+            def _():
+                copy.start()
+
+    send_columns(z)
+    for i in range(depth - 1):
+        g_z[i].wait_recv()
+        block = rg.at[mine, span(downs[i])]
+        g_f.append(put(block, block, across))
+        send_columns(downs[i])
+    for copy in g_f:
+        copy.wait_recv()
+    load_op.wait()
+    hga[g] = contract_cols(rg[...], op[...]).astype(jnp.bfloat16)
+    heads = [put(hga.at[g], hga.at[g], t) for t in (X, Y, Z)]
+    col[g] = rg[:, span(g)]
+    col_f = []
+    for (t, copy) in col_copies:
+        copy.wait_recv()
+        block = col.at[t, mine, :]
+        col_f.append(put(block, block, across))
+    for copy in extras:
+        copy.wait_recv()
+    store(outs_all, outs_out)
+    store(fq_all, fq_out)
+    store(ends_all, ends_out)
+    for copy in col_f:
+        copy.wait_recv()
+    store(col, col_out)
+    for copy in heads:
+        copy.wait_recv()
+    store(hga, hg_out)
+    for copy in sends:
+        copy.wait_send()
+    for copy in stores:
+        copy.wait()
+
+
+def square_call(segs, raw_r, raw_o, route, gain, wg, wu, wd, op, outs, fq, ends):
+    count, width = raw_r.shape
+    feats, heads = wg.shape[1], outs.shape[1]
+    half, quarter = count // CORES, width // segs
+    bf16, f32 = jnp.bfloat16, jnp.float32
+    any_spec = pl.BlockSpec(memory_space=pl.ANY)
+    vmem_spec = pl.BlockSpec(memory_space=pltpu.VMEM)
+    shape = jax.ShapeDtypeStruct
+    flops = 2 * segs * count * width * feats * 8
+    return pl.pallas_call(
+        square_kernel,
+        out_shape=(
+            shape((width, feats), bf16),
+            shape((width, feats), bf16),
+            shape((feats, width), bf16),
+            shape((segs, count, quarter), bf16),
+            shape((segs, count, heads), bf16),
+            shape((segs, count, heads), bf16),
+            shape((segs, count, heads), bf16),
+            shape((segs, 8, 128), f32),
+        ),
+        in_specs=[any_spec, any_spec, vmem_spec, vmem_spec]
+        + [any_spec] * 6
+        + [vmem_spec],
+        out_specs=(any_spec,) * 8,
+        scratch_shapes=[
+            pltpu.VMEM((count, width), bf16),
+            pltpu.VMEM((count, width), bf16),
+            pltpu.VMEM((segs, count, width), bf16),
+            pltpu.VMEM((segs, count, width), bf16),
+            pltpu.VMEM((3, half, width), bf16),
+            pltpu.VMEM((width, feats), bf16),
+            pltpu.VMEM((width, feats), bf16),
+            pltpu.VMEM((feats, width), bf16),
+            pltpu.VMEM((heads, width), bf16),
+            pltpu.VMEM((segs, count, width), bf16),
+            pltpu.VMEM((segs, half, width), bf16),
+            pltpu.VMEM((segs, count, feats), bf16),
+            pltpu.VMEM((segs, count, 2 * feats), bf16),
+            pltpu.VMEM((half, width), bf16),
+            pltpu.VMEM((half, width), bf16),
+            pltpu.VMEM((segs - 1, half, quarter), bf16),
+            pltpu.VMEM((half, quarter), bf16),
+            pltpu.VMEM((half, quarter), bf16),
+            pltpu.VMEM((segs - 1, half, quarter), bf16),
+            pltpu.VMEM((half, quarter), f32),
+            pltpu.VMEM((count, 128), f32),
+            pltpu.VMEM((half, 128), f32),
+            pltpu.VMEM((segs - 1, half, 128), f32),
+            pltpu.VMEM((count, width), bf16),
+            pltpu.VMEM((segs, count, quarter), bf16),
+            pltpu.VMEM((segs, count, heads), bf16),
+            pltpu.VMEM((segs, count, heads), bf16),
+            pltpu.VMEM((segs, count, heads), bf16),
+            pltpu.VMEM((segs, 8, 128), f32),
+            pltpu.VMEM((width, feats), bf16),
+            pltpu.VMEM((width, feats), bf16),
+            pltpu.VMEM((feats, width), bf16),
+            pltpu.SemaphoreType.DMA((72,)),
+            pltpu.SemaphoreType.DMA((72,)),
+            pltpu.SemaphoreType.DMA((8,)),
+            pltpu.SemaphoreType.DMA((8,)),
+        ],
+        compiler_params=pltpu.CompilerParams(
+            collective_id=0, has_side_effects=True, vmem_limit_bytes=66 * 1000 * 1000
+        ),
+        cost_estimate=pl.CostEstimate(flops=flops, bytes_accessed=40000000, transcendentals=0),
+    )(raw_r, raw_o, route, gain, wg, wu, wd, op, outs, fq, ends)
+
+
+def local_square(
+    residual_mid,
+    out_grad,
+    norm_gain,
+    expert_ids,
+    expert_weights,
+    gate_proj,
+    up_proj,
+    down_proj,
+    out_proj,
+    query_rows,
+    key_rows,
+    value_rows,
+    retention_out,
+    log_decay,
+    entry_state,
+):
+    token_count, width = residual_mid.shape
+    segs = lax.axis_size("sp")
+    seg = lax.axis_index("sp")
+    heads_here = log_decay.shape[1]
+    experts = jnp.arange(128, dtype=jnp.int32)
+    route = jnp.sum(
+        jnp.where(
+            expert_ids[:, :, None] == experts[None, None, :], expert_weights[:, :, None], 0.0
+        ),
+        axis=1,
+    )
+
+    def split_heads(rows):
+        return rows.reshape(token_count, heads_here, -1).transpose(1, 0, 2)
+
+    running = jnp.cumsum(log_decay, axis=0).T
+    from_start = jnp.exp(running)
+    head_width = query_rows.shape[1] // heads_here
+    fq = (
+        jnp.repeat(from_start.T, head_width, axis=1) * query_rows.astype(jnp.float32)
+    ).astype(jnp.bfloat16)
+    ends = jnp.zeros((8, 128), jnp.float32).at[:, :heads_here].set(running[:, -1][None, :])
+    gate_grad, up_grad, down_grad, columns, grads, outs, fqs, ends_all = square_call(
+        segs,
+        residual_mid,
+        out_grad,
+        route,
+        norm_gain.reshape(1, width),
+        gate_proj[0],
+        up_proj[0],
+        down_proj[0],
+        out_proj,
+        retention_out,
+        fq,
+        ends,
+    )
+    proj_grad = contract_rows(
+        columns.reshape(segs * token_count, -1), outs.reshape(segs * token_count, -1)
+    )
+    seg_decay = ends_all[:, 0, :heads_here]
+    head_grad = lax.dynamic_index_in_dim(grads, seg, axis=0, keepdims=False)
+    queries = split_heads(query_rows)
+    key_heads = split_heads(key_rows)
+    value_heads = split_heads(value_rows)
+    grad_heads = split_heads(head_grad)
+    key_scale = queries.shape[2] ** (-0.5)
+    to_end = jnp.exp(running[:, -1:] - running)
+    position = jnp.arange(token_count, dtype=jnp.int32)
+    causal = (position[:, None] >= position[None, :])[None]
+    spread = jnp.where(causal, running[:, :, None] - running[:, None, :], 0.0)
+    weights = jnp.where(causal, jnp.exp(spread), 0.0)
+    states = dots(
+        "gthk,gthe->ghke",
+        fqs.reshape(segs, token_count, heads_here, head_width),
+        grads.reshape(segs, token_count, heads_here, head_width),
+    )
+    order = jnp.arange(segs, dtype=jnp.int32)
+    between = (order[None, :] > seg) & (order[None, :] < order[:, None])
+    passed = jnp.exp(jnp.sum(jnp.where(between[:, :, None], seg_decay[None], 0.0), axis=1))
+    passed = jnp.where(order[:, None] > seg, passed, 0.0)
+    later_state = jnp.sum(passed[:, :, None, None] * states, axis=0)
+    entry = entry_state[0]
+    grad_scores = dots("hte,hse->hts", grad_heads, value_heads) * weights
+    key_scores = dots("htk,hsk->hts", queries, key_heads) * weights
+    query_grad = key_scale * (
+        dots("hts,hsk->htk", grad_scores, key_heads)
+        + from_start[:, :, None] * dots("hte,hke->htk", grad_heads, entry)
+    )
+    key_grad = key_scale * (
+        dots("hts,htk->hsk", grad_scores, queries)
+        + to_end[:, :, None] * dots("hse,hke->hsk", value_heads, later_state)
+    )
+    value_grad = key_scale * (
+        dots("hts,hte->hse", key_scores, grad_heads)
+        + to_end[:, :, None] * dots("hsk,hke->hse", key_heads, later_state)
+    )
+
+    def merge_heads(heads_rows):
+        return heads_rows.transpose(1, 0, 2).reshape(token_count, -1).astype(jnp.bfloat16)
+
+    return (
+        gate_grad[None],
+        up_grad[None],
+        down_grad[None],
+        proj_grad,
+        merge_heads(query_grad),
+        merge_heads(key_grad),
+        merge_heads(value_grad),
+    )
+
+
 def solution(mesh):
     segs, split = mesh.shape["sp"], mesh.shape["tp"]
     fine = Mesh(mesh.devices.reshape(segs, split // CORES, CORES), ("sp", "z", "core"))
@@ -233,8 +811,9 @@
         P("sp", tp),
         P("sp", tp, None, None),
     )
+    fast = segs == 4 and split == segs * CORES
     return jax.shard_map(
-        local,
+        local_square if fast else local_general,
         mesh=fine,
         in_specs=placed,
         out_specs=(

time: 295 us -> 151 us (0.51)
  waiting for transfers between devices: 167 us -> 0 us
  Pallas kernels: 0 us -> 126 us
  matrix products: 57.6 us -> 6 us
  blocking collectives: 19.3 us -> 0 us
  between operations: 15.3 us -> 0.81 us
  starting transfers between devices: 9.89 us -> 0 us
  other arithmetic: 11.7 us -> 5.46 us
    pallas_call x0 -> x1, Pallas kernels: none -> 126 us  [square_call(): pl.pallas_call(square_kernel, out_shape=(shape((width, feats), bf16), sha...]
    all_gather x5 -> x0, waiting for transfers between devices: 107 us -> none  [the longest x1 41.1 us: local(): lax.all_gather(rows_of(out_grad, core * half, half), 'sp')]
    unnamed x8 -> x0, waiting for transfers between devices: 40.6 us -> none
    dot_general x7 -> x1, matrix products: 30.9 us -> 2.33 us  [contract_rows(): lax.dot_general(left, right, (((0,), (0,)), ((), ())), preferred_element_...]
    dot_general x11 -> x0, matrix products: 22.1 us -> none  [the longest x7 13.4 us: contract_cols(): lax.dot_general(left, right, (((1,), (1,)), ((), ())), preferred_element_...]
    reduce_scatter x1 -> x0, waiting for transfers between devices: 18.9 us -> none  [local(): lax.psum_scatter(part_seg.reshape(depth, share, width), 'z', scatter_dime...]
    unnamed x1 -> x0, blocking collectives: 10.3 us -> none
    all_gather x1 -> x0, blocking collectives: 9.01 us -> none  [local(): outs = lax.all_gather(retention_out, 'sp')]
  transfers between devices with their start and end apart: 11 -> 0, of which waited for: 6 -> 0; matrix products, arithmetic and copies ran while one was open for 20% -> 0% of each run, Pallas kernels for 0% -> 0%
where the time goes in v1:
time: 151 us; the launch traced here: 150 us
  Pallas kernels  126 us (83%)
  local copies, waits for them, and re-layouts  12.1 us (8%)
  matrix products  6 us (4%)
  other arithmetic  5.46 us (4%)
    pallas_call x1, Pallas kernels, square_call(): pl.pallas_call(square_kernel, out_shape=(shape((width, feats), bf16), sha...  126 us
    unnamed x24, local copies, waits for them, and re-layouts  6.2 us
    dot_general x8, matrix products, dots(): jnp.einsum(spec, left.astype(jnp.bfloat16), right.astype(jnp.bfloat16), p...  3.67 us

profile of v1, /device:TPU:27, one launch (start us, length us, event | category | flops | bytes accessed | tf_op | source)
XLA Modules:
  0.0 150.5 jit_solution(10850709437459405032)
XLA Ops:
  0.6 0.7 pad.6
  1.3 0.6 reduce-window.6
  1.9 0.2 slice_reduce_fusion
  2.1 0.2 reduce-window.9
  2.3 0.1 add_bitcast_fusion
  2.4 0.2 slice_reduce_fusion.1
  2.6 0.1 subtract_exponential_fusion
  2.6 0.1 copy.109
  2.8 0.2 broadcast_in_dim.101.clone
  3.0 1.6 %multiply_convert_fusion.fq_hbm = bf16[160,512]{1,0:T(8,128)(2,1)} fusion(f32[160,512]{1,0:T(8,128)S(1)} %bitcast.136, bf16[160,512]{1,0:T(8,128)(2,1)} %param.26), kind=kLoop, calls=%fused_computation.32 | loop fusion | flops 245760 | bytes 655360 | tf_op jit(solution)/shard_map/convert_element_type | solution.py:722
  4.7 0.6 compare_reduce_fusion
  5.3 0.6 broadcast_select_fusion
  6.0 0.6 scatter.8.ends_ref
  6.6 1.5 select_reduce_fusion.route_ref
  8.0 126.1 %shard_map.198 = (bf16[4096,256]{1,0:T(8,128)(2,1)}, bf16[4096,256]{1,0:T(8,128)(2,1)}, bf16[256,4096]{1,0:T(8,128)(2,1)}, bf16[4,160,1024]{2,1,0:T(8,128)(2,1)}...) custom-call(bf16[160,4096]{1,0:T(8,128)(2,1)} %raw_r_hbm.1, ...), custom_call_target="tpu_custom_call" | custom-call | flops 10737418240 | bytes 40000000 | tf_op jit(solution)/shard_map/pallas_call | solution.py:624
  134.2 0.0 copy-start.3
  134.2 0.0 copy-start.4
  134.2 0.8 slice.33
  135.0 0.1 copy.100
  135.1 0.1 select_reduce_fusion.1
  135.2 0.1 copy.101
  135.3 1.9 %multiply_reduce_fusion = bf16[2,256,256]{2,1,0:T(8,128)(2,1)S(1)} fusion(f32[4,2]{1,0:T(4,128)S(1)} %copy.101, bf16[4,20,2,8,256]{4,3,2,1,0:T(8,128)(2,1)} %bitcast.147, bf16[4,20,2,8,256]{4,3,2,1,0:T(8,128)(2,1)} %bitcast.157), kind=kOutput, calls=%fused_computation | convolution fusion | flops 168689664 | bytes 1572896 | tf_op jit(solution)/shard_map/gthk,gthe->ghke/dot_general | solution.py:36
  137.1 0.0 copy-start.6
  137.2 1.0 constant_dynamic-slice_fusion
  138.2 0.0 copy-done.3
  138.2 0.0 copy-done.4
  138.2 0.5 convolution_bitcast_fusion.4
  138.7 0.2 fusion.16
  138.9 0.0 copy-start.5
  138.9 0.7 copy.117
  139.6 0.0 copy-done.6
  139.6 0.2 fusion.9
  139.8 0.0 copy-start.8
  139.8 0.2 convolution_bitcast_fusion.5
  140.1 0.2 fusion.15
  140.3 0.7 copy.116
  141.0 0.2 convolution_bitcast_fusion.6
  141.2 0.0 copy-done.5
  141.2 0.2 fusion.14
  141.4 0.7 copy.115
  142.1 0.0 copy-done.7
  142.1 0.0 copy-done.8
  142.1 2.3 %convolution_bitcast_fusion = f32[1024,512]{1,0:T(8,128)} fusion(bf16[4,160,1024]{2,1,0:T(8,128)(2,1)S(1)} %copy-done.7, bf16[4,160,512]{2,1,0:T(8,128)(2,1)S(1)} %copy-done.8), kind=kOutput, calls=%fused_computation.1 | convolution fusion | flops 671088640 | bytes 4063232 | tf_op jit(solution)/shard_map/dot_general | solution.py:24
  144.5 1.3 copy.175
  145.8 1.0 copy-done.1
  146.8 1.3 copy.176
  148.1 1.0 copy-done
  149.2 1.3 copy.177
  (15 shorter events, 0.2 us)
Async XLA Ops:
  134.2 4.0 %copy-start.3 = (bf16[160,512]{1,0:T(8,128)(2,1)S(1)}, bf16[160,512]{1,0:T(8,128)(2,1)}, u32[]{:S(2)}) copy-start(bf16[160,512]{1,0:T(8,128)(2,1)} %param.26) | copy-start | bytes 491524
  134.2 4.0 %copy-start.4 = (bf16[160,512]{1,0:T(8,128)(2,1)S(1)}, bf16[160,512]{1,0:T(8,128)(2,1)}, u32[]{:S(2)}) copy-start(bf16[160,512]{1,0:T(8,128)(2,1)} %param.27) | copy-start | bytes 491524
  137.1 2.4 %copy-start.6 = (bf16[160,512]{1,0:T(8,128)(2,1)S(1)}, bf16[160,512]{1,0:T(8,128)(2,1)}, u32[]{:S(2)}) copy-start(bf16[160,512]{1,0:T(8,128)(2,1)} %param.28) | copy-start | bytes 491524
  138.9 2.3 %copy-start.5 = (f32[1,2,256,256]{3,2,1,0:T(8,128)S(1)}, f32[1,2,256,256]{3,2,1,0:T(8,128)}, u32[]{:S(2)}) copy-start(f32[1,2,256,256]{3,2,1,0:T(8,128)} %param.31) | copy-start | bytes 1572868
  139.8 2.3 %copy-start.7 = (bf16[4,160,1024]{2,1,0:T(8,128)(2,1)S(1)}, bf16[4,160,1024]{2,1,0:T(8,128)(2,1)}, u32[]{:S(2)}) copy-start(bf16[4,160,1024]{2,1,0:T(8,128)(2,1)} %get-tuple-element.30) | copy-start | bytes 3932164
  139.8 2.3 %copy-start.8 = (bf16[4,160,512]{2,1,0:T(8,128)(2,1)S(1)}, bf16[4,160,512]{2,1,0:T(8,128)(2,1)}, u32[]{:S(2)}) copy-start(bf16[4,160,512]{2,1,0:T(8,128)(2,1)} %get-tuple-element.31) | copy-start | bytes 1966084
  142.1 2.3 %copy-start.2 = (bf16[4096,256]{1,0:T(8,128)(2,1)S(1)}, bf16[4096,256]{1,0:T(8,128)(2,1)}, u32[]{:S(2)}) copy-start(bf16[4096,256]{1,0:T(8,128)(2,1)} %get-tuple-element.27) | copy-start | bytes 6291460
  144.5 2.3 %copy-start.1 = (bf16[4096,256]{1,0:T(8,128)(2,1)S(1)}, bf16[4096,256]{1,0:T(8,128)(2,1)}, u32[]{:S(2)}) copy-start(bf16[4096,256]{1,0:T(8,128)(2,1)} %get-tuple-element.28) | copy-start | bytes 6291460
  146.8 2.3 %copy-start = (bf16[256,4096]{1,0:T(8,128)(2,1)S(1)}, bf16[256,4096]{1,0:T(8,128)(2,1)}, u32[]{:S(2)}) copy-start(bf16[256,4096]{1,0:T(8,128)(2,1)} %get-tuple-element.29) | copy-start | bytes 6291460

commit v2 on v1

--- a/solution.py
+++ b/solution.py
@@ -1,5 +1,3 @@
-import functools
-
 import jax
 import jax.numpy as jnp
 from jax import lax
@@ -217,21 +215,23 @@
 
 
 ROWS = 16
+VMEM_LIMIT = 66 * 1000 * 1000
 MESH_ID = pl.DeviceIdType.MESH
 
 
 def square_kernel(
     raw_r_hbm,
     raw_o_hbm,
-    route_ref,
+    ids_ref,
+    scale_ref,
+    decay_ref,
     gain_ref,
     wg_hbm,
     wu_hbm,
     wd_hbm,
     op_hbm,
     outs_hbm,
-    fq_hbm,
-    ends_ref,
+    query_hbm,
     gate_out,
     up_out,
     down_out,
@@ -253,14 +253,21 @@
     pin,
     hid,
     back,
+    pre,
+    hgrad,
+    query,
     rx,
     ry,
+    rdd,
     rz1,
     sd,
     rd,
     rz2,
-    wz,
     inv,
+    route,
+    means,
+    mrow,
+    mland,
     msend,
     mz,
     rg,
@@ -322,6 +329,9 @@
         copy.start()
         return copy
 
+    def line_put(block):
+        return [put(block, block, target) for target in along]
+
     loads = []
 
     def load(src, dst):
@@ -337,12 +347,12 @@
         copy.start()
         stores.append(copy)
 
+    load_r = load(raw_r_hbm, raw_r)
     load_o = load(raw_o_hbm, raw_o)
-    load_r = load(raw_r_hbm, raw_r)
     load_w = [load(wg_hbm, wg), load(wu_hbm, wu), load(wd_hbm, wd)]
     load_op = load(op_hbm, op)
-    load_outs = load(outs_hbm, outs_all.at[g])
-    load_fq = load(fq_hbm, fq_all.at[g])
+    load_outs = load(outs_hbm, outs_all.at[0])
+    load_query = load(query_hbm, query)
 
     X, Y, Z = dev(gx, z, c), dev(gy, z, c), dev(gd, z, c)
     across = dev(g, z, 1 - c)
@@ -351,12 +361,24 @@
     for target in [X, Y, Z, across] + along:
         pl.semaphore_signal(barrier, inc=1, device_id=target, device_id_type=MESH_ID)
 
-    lanes = lax.broadcasted_iota(jnp.int32, (ROWS, 128), 1)
-
-    def weigh(base, rows, expert, write):
+    kinds = (g, gd, gx, gy)
+    which = lax.broadcasted_iota(jnp.int32, (8, count), 0)
+    table = jnp.zeros((8, count), jnp.float32)
+    for k, expert in enumerate(kinds):
+        chosen = jnp.where(ids_ref[...] == expert, scale_ref[...], 0.0)
+        table = jnp.where(which == k, jnp.sum(chosen, axis=0, keepdims=True), table)
+    unit = lax.broadcasted_iota(jnp.int32, (8, 128), 0) == lax.broadcasted_iota(
+        jnp.int32, (8, 128), 1
+    )
+    exact = dict(preferred_element_type=jnp.float32, precision=lax.Precision.HIGHEST)
+    route[...] = lax.dot_general(
+        table, unit.astype(jnp.float32), (((0,), (0,)), ((), ())), **exact
+    )
+
+    def weigh(base, rows, kind, write):
         def step(i, carry):
             r = pl.ds(pl.multiple_of(base + i * ROWS, ROWS), ROWS)
-            w = jnp.sum(jnp.where(lanes == expert, route_ref[r, :], 0.0), axis=1, keepdims=True)
+            w = route[r, kind : kind + 1]
             write(i, r, (w * raw_o[r, :].astype(jnp.float32)).astype(jnp.bfloat16))
             return carry
 
@@ -369,7 +391,7 @@
         return write
 
     def own_write(i, r, value):
-        og[g, r, :] = value
+        og[0, r, :] = value
 
     def normalize(base, rows):
         def step(i, carry):
@@ -377,78 +399,138 @@
             wide = raw_r[r, :].astype(jnp.float32)
             inverse = lax.rsqrt(jnp.mean(wide * wide, axis=1, keepdims=True) + NORM_EPSILON)
             inv[r, :] = jnp.broadcast_to(inverse, (ROWS, 128))
-            rin[g, r, :] = (wide * inverse * gain_ref[...]).astype(jnp.bfloat16)
+            rin[0, r, :] = (wide * inverse * gain_ref[...]).astype(jnp.bfloat16)
             return carry
 
         lax.fori_loop(0, rows // ROWS, step, 0)
 
-    load_o.wait()
-    weigh(c * half, half, gd, stage(2))
-    pl.semaphore_wait(barrier, 4 + len(along))
-    d_o = put(stg.at[2, :, span(z)], og.at[g, mine, span(z)], Z)
     load_r.wait()
     normalize(c * half, half)
-    d_n = put(rin.at[g, mine, span(z)], rin.at[g, mine, span(z)], Z)
-    x_n = put(rin.at[g, mine, :], rin.at[g, mine, :], X)
-    y_n = put(rin.at[g, mine, :], rin.at[g, mine, :], Y)
-    weigh(c * half, half, gx, stage(0))
-    x_o = put(stg.at[0], og.at[g, mine, :], X)
-    weigh(c * half, half, gy, stage(1))
-    y_o = put(stg.at[1], og.at[g, mine, :], Y)
+    pl.semaphore_wait(barrier, 4 + len(along))
+    d_n = put(rin.at[0, mine, span(z)], rin.at[1, mine, span(z)], Z)
+    load_o.wait()
+    weigh(c * half, half, 1, stage(2))
+    d_o = put(stg.at[2, :, span(z)], og.at[1, mine, span(z)], Z)
+    x_n = put(rin.at[0, mine, :], rin.at[2, mine, :], X)
+    y_n = put(rin.at[0, mine, :], rin.at[3, mine, :], Y)
+    weigh(c * half, half, 2, stage(0))
+    x_o = put(stg.at[0], og.at[2, mine, :], X)
+    weigh(c * half, half, 3, stage(1))
+    y_o = put(stg.at[1], og.at[3, mine, :], Y)
+
+    def spread(buf):
+        block = buf.at[1, mine, span(z)]
+        return line_put(block) + [put(block, block, across)]
+
+    def collect(buf, copies, i):
+        copies[i].wait_recv()
+        block = buf.at[1, mine, span(downs[i])]
+        return put(block, block, across)
+
+    def forward(buf, slot):
+        block = buf.at[slot, mine, :]
+        return put(block, block, across)
+
+    d_n.wait_recv()
+    n_spread = spread(rin)
     normalize((1 - c) * half, half)
-    weigh(0, count, g, own_write)
-
-    def spread(buf):
-        block = buf.at[gd, mine, span(z)]
-        return [put(block, block, t) for t in along] + [put(block, block, across)]
-
+    weigh(0, count, 0, own_write)
     d_o.wait_recv()
     o_spread = spread(og)
-    d_n.wait_recv()
-    n_spread = spread(rin)
+
+    heads_here = decay_ref.shape[0]
+    head_width = query.shape[1] // heads_here
+    later = lax.broadcasted_iota(jnp.int32, (count, count), 0)
+    lower = (later >= lax.broadcasted_iota(jnp.int32, (count, count), 1)).astype(jnp.float32)
+    running = lax.dot_general(lower, decay_ref[...], (((1,), (1,)), ((), ())), **exact)
+    load_query.wait()
+    for h in range(heads_here):
+        cols = slice(h * head_width, (h + 1) * head_width)
+        fq_all[0, :, cols] = (
+            jnp.exp(running[:, h : h + 1]) * query[:, cols].astype(jnp.float32)
+        ).astype(jnp.bfloat16)
+    ends_all[0] = jnp.zeros((8, 128), jnp.float32)
+    ends_all[0, :, :heads_here] = jnp.broadcast_to(running[count - 1 :, :], (8, heads_here))
+    load_outs.wait()
+    extras = []
+    for slot, target in ((1, Z), (2, X), (3, Y)):
+        for buf in (ends_all, fq_all):
+            extras.append(put(buf.at[0], buf.at[slot], target))
 
     for copy in load_w:
         copy.wait()
 
-    def expert(s):
-        gate_pre = jnp.dot(rin[s], wg[...], preferred_element_type=jnp.float32)
-        up_pre = jnp.dot(rin[s], wu[...], preferred_element_type=jnp.float32)
-        hidden, pullback = jax.vjp(activate, gate_pre, up_pre)
-        gate_back, up_back = pullback(contract_cols(og[s], wd[...]))
-        gate_back = gate_back.astype(jnp.bfloat16)
-        up_back = up_back.astype(jnp.bfloat16)
+    def gates(slots, rows):
+        lhs = rin[slots].reshape(rows, width)
+        pre[slots, :, :feats] = jnp.dot(
+            lhs, wg[...], preferred_element_type=jnp.float32
+        ).reshape(-1, count, feats)
+        pre[slots, :, feats:] = jnp.dot(
+            lhs, wu[...], preferred_element_type=jnp.float32
+        ).reshape(-1, count, feats)
+
+    def hidden_grads(slots, rows):
+        lhs = og[slots].reshape(rows, width)
+        hgrad[slots] = contract_cols(lhs, wd[...]).reshape(-1, count, feats)
+
+    def activations(s):
+        hidden, pullback = jax.vjp(activate, pre[s, :, :feats], pre[s, :, feats:])
+        gate_back, up_back = pullback(hgrad[s])
+        both = gate_back * pre[s, :, :feats] + up_back * pre[s, :, feats:]
+        mrow[0, s] = lax.dot_general(
+            jnp.ones((8, feats), jnp.float32), both, (((1,), (1,)), ((), ())), **exact
+        )
         hid[s] = hidden.astype(jnp.bfloat16)
-        back[s, :, :feats] = gate_back
-        back[s, :, feats:] = up_back
-
-        def step(n, carry):
-            rows = pl.ds(pl.multiple_of(n * quarter, 128), quarter)
-            piece = contract_cols(back[s, :, :feats], wg[rows, :]) + contract_cols(
-                back[s, :, feats:], wu[rows, :]
-            )
-            part[s, :, rows] = piece.astype(jnp.bfloat16)
+        back[s, :, :feats] = gate_back.astype(jnp.bfloat16)
+        back[s, :, feats:] = up_back.astype(jnp.bfloat16)
+
+    def part_step(slots, rows, cols):
+        lhs = back[slots].reshape(rows, 2 * feats)
+        piece = contract_cols(lhs[:, :feats], wg[cols, :]) + contract_cols(
+            lhs[:, feats:], wu[cols, :]
+        )
+        part[slots, :, cols] = piece.astype(jnp.bfloat16).reshape(-1, count, quarter)
+
+    def pair_step(s, cols):
+        def step(i, carry):
+            r = pl.ds(pl.multiple_of(c * half + i * ROWS, ROWS), ROWS)
+            q = pl.ds(pl.multiple_of(i * ROWS, ROWS), ROWS)
+            total = part[s, r, cols].astype(jnp.float32) + pin[s, q, cols].astype(jnp.float32)
+            part[s, r, cols] = total.astype(jnp.bfloat16)
             return carry
 
-        lax.fori_loop(0, depth, step, 0)
-        return put(part.at[s, theirs, :], pin.at[s], across)
-
-    swap_own = expert(g)
-
+        lax.fori_loop(0, half // ROWS, step, 0)
+
+    gates(slice(0, 1), count)
+    hidden_grads(slice(0, 1), count)
+    activations(0)
+
+    def own_step(n, carry):
+        part_step(slice(0, 1), count, span(n))
+        return carry
+
+    lax.fori_loop(0, depth, own_step, 0)
+    swap_own = put(part.at[0, theirs, :], pin.at[0], across)
+
+    rest = (segs - 1) * count
     x_n.wait_recv()
-    f = [put(rin.at[gx, mine, :], rin.at[gx, mine, :], across)]
+    f = [forward(rin, 2)]
     y_n.wait_recv()
-    f.append(put(rin.at[gy, mine, :], rin.at[gy, mine, :], across))
+    f.append(forward(rin, 3))
     for i in range(depth - 1):
-        for buf, group in ((og, o_spread), (rin, n_spread)):
-            group[i].wait_recv()
-            block = buf.at[gd, mine, span(downs[i])]
-            f.append(put(block, block, across))
+        f.append(collect(rin, n_spread, i))
+    n_spread[-1].wait_recv()
+    for copy in f:
+        copy.wait_recv()
+    gates(slice(1, segs), rest)
+    f = []
+    for i in range(depth - 1):
+        f.append(collect(og, o_spread, i))
     x_o.wait_recv()
-    f.append(put(og.at[gx, mine, :], og.at[gx, mine, :], across))
+    f.append(forward(og, 2))
     y_o.wait_recv()
-    f.append(put(og.at[gy, mine, :], og.at[gy, mine, :], across))
+    f.append(forward(og, 3))
     o_spread[-1].wait_recv()
-    n_spread[-1].wait_recv()
     for copy in f:
         copy.wait_recv()
 
@@ -466,15 +548,48 @@
 
         lax.fori_loop(0, half // ROWS, step, 0)
 
-    swap_d = expert(gd)
-    swap_x = expert(gx)
-    pair(gd, swap_d)
-    d_z = [put(part.at[gd, mine, span(ups[i])], rz1.at[i], along[i]) for i in range(depth - 1)]
-    swap_y = expert(gy)
-    pair(gx, swap_x)
-    x_p = put(part.at[gx, mine, :], rx, X)
-    pair(gy, swap_y)
-    y_p = put(part.at[gy, mine, :], ry, Y)
+    line_rows = rz1.shape[1]
+    on_line = pl.ds(pl.multiple_of(c * half, ROWS), line_rows)
+    direct = pl.ds(pl.multiple_of(c * half + line_rows, ROWS), half - line_rows)
+    order = [span(q) for q in ups] + [span(z)]
+    swaps, x_p, y_p, dd_p, d_z = [], [], [], [], []
+
+    def advance(n):
+        cols = order[n]
+        for copy in swaps[n]:
+            copy.wait_recv()
+        pair_step(2, cols)
+        x_p.append(put(part.at[2, mine, cols], rx.at[:, cols], X))
+        pair_step(3, cols)
+        y_p.append(put(part.at[3, mine, cols], ry.at[:, cols], Y))
+        pair_step(1, cols)
+        dd_p.append(put(part.at[1, direct, cols], rdd.at[:, cols], Z))
+        if n < depth - 1:
+            d_z.append(put(part.at[1, on_line, cols], rz1.at[n], along[n]))
+
+    hidden_grads(slice(1, segs), rest)
+    for slot in range(1, segs):
+        activations(slot)
+    m_pair = put(mrow.at[0], mrow.at[1], across)
+    for n, cols in enumerate(order):
+        part_step(slice(1, segs), rest, cols)
+        swaps.append(
+            [
+                put(part.at[slot, theirs, cols], pin.at[slot, :, cols], across)
+                for slot in (2, 3, 1)
+            ]
+        )
+        if n == 1:
+            m_pair.wait_recv()
+            mrow[2] = mrow[0] + mrow[1]
+            m_side = [
+                put(mrow.at[2, slot], mland.at[slot - 1], target)
+                for slot, target in ((1, Z), (2, X), (3, Y))
+            ]
+        if n >= 2:
+            advance(n - 2)
+    for n in range(depth - 2, depth):
+        advance(n)
 
     def weight_step(n, carry):
         cols = pl.ds(pl.multiple_of(n * 512, 128), 512)
@@ -487,42 +602,59 @@
     store(gout, gate_out)
     store(uout, up_out)
 
-    def z_sum(own, landed, write, more=None):
-        for copy in landed[0]:
-            copy.wait_recv()
+    def line_step(i, carry):
+        q = pl.ds(pl.multiple_of(i * ROWS, ROWS), ROWS)
+        r = pl.ds(pl.multiple_of(c * half + i * ROWS, ROWS), ROWS)
+        total = part[1, r, span(z)].astype(jnp.float32)
+        for k in range(depth - 1):
+            total = total + rz1[k, q, :].astype(jnp.float32)
+        sd[q, :] = total.astype(jnp.bfloat16)
+        return carry
+
+    swap_own.wait_recv()
+    own_z = []
+    for n, cols in enumerate(order):
+        if n == depth - 1:
+            for copy in d_z:
+                copy.wait_recv()
+            lax.fori_loop(0, line_rows // ROWS, line_step, 0)
+            d_p = put(sd, rd, Z)
+            for slot, target in ((1, Z), (2, X), (3, Y)):
+                extras.append(put(outs_all.at[0], outs_all.at[slot], target))
+        for copies in (x_p, y_p, dd_p):
+            copies[n].wait_recv()
 
         def step(i, carry):
+            r = pl.ds(pl.multiple_of(c * half + i * ROWS, ROWS), ROWS)
             q = pl.ds(pl.multiple_of(i * ROWS, ROWS), ROWS)
+            total = part[0, r, cols].astype(jnp.float32)
+            for ref in (pin.at[0], rx, ry):
+                total = total + ref[q, cols].astype(jnp.float32)
+            part[0, r, cols] = total.astype(jnp.bfloat16)
+            return carry
+
+        def direct_step(i, carry):
             r = pl.ds(pl.multiple_of(c * half + i * ROWS, ROWS), ROWS)
-            total = part[own, r, span(z)].astype(jnp.float32)
-            for k in range(depth - 1):
-                total = total + landed[1][k, q, :].astype(jnp.float32)
-            if more is not None:
-                total = total + more[q, :].astype(jnp.float32)
-            write(q, r, total)
+            q = pl.ds(pl.multiple_of(i * ROWS, ROWS), ROWS)
+            u = pl.ds(pl.multiple_of(i * ROWS - line_rows, ROWS), ROWS)
+            total = part[0, r, cols].astype(jnp.float32)
+            for ref in (pin.at[0], rx, ry):
+                total = total + ref[q, cols].astype(jnp.float32)
+            total = total + rdd[u, cols].astype(jnp.float32)
+            part[0, r, cols] = total.astype(jnp.bfloat16)
             return carry
 
-        lax.fori_loop(0, half // ROWS, step, 0)
-
-    def write_sd(q, r, total):
-        sd[q, :] = total.astype(jnp.bfloat16)
-
-    z_sum(gd, (d_z, rz1), write_sd)
-    d_p = put(sd, rd, Z)
-
-    load_outs.wait()
-    load_fq.wait()
-    extras = []
-    for target in (X, Y, Z):
-        extras.append(put(fq_all.at[g], fq_all.at[g], target))
-        extras.append(put(ends_ref, ends_all.at[g], target))
-        extras.append(put(outs_all.at[g], outs_all.at[g], target))
-    ends_all[g] = ends_ref[...]
-
-    x_p.wait_recv()
-    y_p.wait_recv()
-    pair(g, swap_own, (rx, ry))
-    own_z = [put(part.at[g, mine, span(ups[i])], rz2.at[i], along[i]) for i in range(depth - 1)]
+        lax.fori_loop(0, line_rows // ROWS, step, 0)
+        lax.fori_loop(line_rows // ROWS, half // ROWS, direct_step, 0)
+        if n == 0:
+            total = mrow[2, 0]
+            for k, copy in enumerate(m_side):
+                copy.wait_recv()
+                total = total + mland[k]
+            msend[...] = total
+            m_z = [put(msend, mz.at[i], along[i]) for i in range(depth - 1)]
+        if n < depth - 1:
+            own_z.append(put(part.at[0, mine, cols], rz2.at[n], along[n]))
 
     def down_step(n, carry):
         cols = pl.ds(pl.multiple_of(n * 512, 128), 512)
@@ -537,42 +669,51 @@
 
     d_p.wait_recv()
 
-    def write_m(q, r, total):
-        weighted = gain_ref[:, span(z)] * total
-        scaled = raw_r[r, span(z)].astype(jnp.float32) * inv[r, 0:1]
-        inner = jnp.sum(scaled * weighted, axis=1, keepdims=True)
-        msend[q, :] = jnp.broadcast_to(inner, (ROWS, 128))
-        wz[q, :] = weighted
-
-    z_sum(g, (own_z, rz2), write_m, rd)
-    m_z = [put(msend, mz.at[i], along[i]) for i in range(depth - 1)]
-    for copy in m_z:
+    total = msend[...]
+    for k, copy in enumerate(m_z):
         copy.wait_recv()
-
-    def resid_step(i, carry):
+        total = total + mz[k]
+    first = lax.broadcasted_iota(jnp.int32, (8, 128), 0) == 0
+    means[...] = lax.dot_general(
+        total / width, first.astype(jnp.float32), (((0,), (0,)), ((), ())), **exact
+    )
+    for copy in own_z:
+        copy.wait_recv()
+
+    def resid_step(i, u):
         q = pl.ds(pl.multiple_of(i * ROWS, ROWS), ROWS)
         r = pl.ds(pl.multiple_of(c * half + i * ROWS, ROWS), ROWS)
+        total = part[0, r, span(z)].astype(jnp.float32)
+        for k in range(depth - 1):
+            total = total + rz2[k, q, :].astype(jnp.float32)
+        if u is not None:
+            total = total + rd[q, :].astype(jnp.float32)
+        weighted = gain_ref[:, span(z)] * total
         inverse = inv[r, 0:1]
         scaled = raw_r[r, span(z)].astype(jnp.float32) * inverse
-        inner = msend[q, 0:1]
-        for k in range(depth - 1):
-            inner = inner + mz[k, q, 0:1]
-        inner = inner / width
-        grad = raw_o[r, span(z)].astype(jnp.float32) + inverse * (wz[q, :] - scaled * inner)
+        grad = raw_o[r, span(z)].astype(jnp.float32) + inverse * (weighted - scaled * means[r, 0:1])
         rg[r, span(z)] = grad.astype(jnp.bfloat16)
+
+    def resid_line(i, carry):
+        resid_step(i, True)
         return carry
 
-    lax.fori_loop(0, half // ROWS, resid_step, 0)
+    def resid_direct(i, carry):
+        resid_step(i, None)
+        return carry
+
+    lax.fori_loop(0, line_rows // ROWS, resid_line, 0)
+    lax.fori_loop(line_rows // ROWS, half // ROWS, resid_direct, 0)
     block = rg.at[mine, span(z)]
-    g_z = [put(block, block, t) for t in along]
+    g_z = line_put(block)
     g_f = [put(block, block, across)]
     col_copies = [
-        (t, remote(rg.at[mine, span(t)], col.at[g, mine, :], target))
-        for t, target in ((gx, X), (gy, Y), (gd, Z))
+        (t, slot, remote(rg.at[mine, span(t)], col.at[slot, mine, :], target))
+        for t, slot, target in ((gd, 1, Z), (gx, 2, X), (gy, 3, Y))
     ]
 
     def send_columns(q):
-        for t, copy in col_copies:
+        for t, _, copy in col_copies:
 
             @pl.when(q == t)
             def _():
@@ -587,14 +728,13 @@
     for copy in g_f:
         copy.wait_recv()
     load_op.wait()
-    hga[g] = contract_cols(rg[...], op[...]).astype(jnp.bfloat16)
-    heads = [put(hga.at[g], hga.at[g], t) for t in (X, Y, Z)]
-    col[g] = rg[:, span(g)]
+    hga[0] = contract_cols(rg[...], op[...]).astype(jnp.bfloat16)
+    heads = [put(hga.at[0], hga.at[slot], t) for slot, t in ((1, Z), (2, X), (3, Y))]
+    col[0] = rg[:, span(g)]
     col_f = []
-    for (t, copy) in col_copies:
+    for _, slot, copy in col_copies:
         copy.wait_recv()
-        block = col.at[t, mine, :]
-        col_f.append(put(block, block, across))
+        col_f.append(forward(col, slot))
     for copy in extras:
         copy.wait_recv()
     store(outs_all, outs_out)
@@ -612,10 +752,11 @@
         copy.wait()
 
 
-def square_call(segs, raw_r, raw_o, route, gain, wg, wu, wd, op, outs, fq, ends):
+def square_call(segs, raw_r, raw_o, ids, scale, decay, gain, wg, wu, wd, op, outs, query):
     count, width = raw_r.shape
     feats, heads = wg.shape[1], outs.shape[1]
     half, quarter = count // CORES, width // segs
+    line = half * 3 // 5 // ROWS * ROWS
     bf16, f32 = jnp.bfloat16, jnp.float32
     any_spec = pl.BlockSpec(memory_space=pl.ANY)
     vmem_spec = pl.BlockSpec(memory_space=pltpu.VMEM)
@@ -633,9 +774,7 @@
             shape((segs, count, heads), bf16),
             shape((segs, 8, 128), f32),
         ),
-        in_specs=[any_spec, any_spec, vmem_spec, vmem_spec]
-        + [any_spec] * 6
-        + [vmem_spec],
+        in_specs=[any_spec] * 2 + [vmem_spec] * 4 + [any_spec] * 6,
         out_specs=(any_spec,) * 8,
         scratch_shapes=[
             pltpu.VMEM((count, width), bf16),
@@ -651,16 +790,23 @@
             pltpu.VMEM((segs, half, width), bf16),
             pltpu.VMEM((segs, count, feats), bf16),
             pltpu.VMEM((segs, count, 2 * feats), bf16),
+            pltpu.VMEM((segs, count, 2 * feats), f32),
+            pltpu.VMEM((segs, count, feats), f32),
+            pltpu.VMEM((count, heads), bf16),
             pltpu.VMEM((half, width), bf16),
             pltpu.VMEM((half, width), bf16),
+            pltpu.VMEM((half - line, width), bf16),
+            pltpu.VMEM((segs - 1, line, quarter), bf16),
+            pltpu.VMEM((line, quarter), bf16),
+            pltpu.VMEM((line, quarter), bf16),
             pltpu.VMEM((segs - 1, half, quarter), bf16),
-            pltpu.VMEM((half, quarter), bf16),
-            pltpu.VMEM((half, quarter), bf16),
-            pltpu.VMEM((segs - 1, half, quarter), bf16),
-            pltpu.VMEM((half, quarter), f32),
             pltpu.VMEM((count, 128), f32),
-            pltpu.VMEM((half, 128), f32),
-            pltpu.VMEM((segs - 1, half, 128), f32),
+            pltpu.VMEM((count, 128), f32),
+            pltpu.VMEM((count, 128), f32),
+            pltpu.VMEM((3, segs, 8, count), f32),
+            pltpu.VMEM((segs - 1, 8, count), f32),
+            pltpu.VMEM((8, count), f32),
+            pltpu.VMEM((segs - 1, 8, count), f32),
             pltpu.VMEM((count, width), bf16),
             pltpu.VMEM((segs, count, quarter), bf16),
             pltpu.VMEM((segs, count, heads), bf16),
@@ -670,16 +816,190 @@
             pltpu.VMEM((width, feats), bf16),
             pltpu.VMEM((width, feats), bf16),
             pltpu.VMEM((feats, width), bf16),
-            pltpu.SemaphoreType.DMA((72,)),
-            pltpu.SemaphoreType.DMA((72,)),
+            pltpu.SemaphoreType.DMA((96,)),
+            pltpu.SemaphoreType.DMA((96,)),
             pltpu.SemaphoreType.DMA((8,)),
             pltpu.SemaphoreType.DMA((8,)),
         ],
         compiler_params=pltpu.CompilerParams(
-            collective_id=0, has_side_effects=True, vmem_limit_bytes=66 * 1000 * 1000
+            collective_id=0, has_side_effects=True, vmem_limit_bytes=VMEM_LIMIT
         ),
         cost_estimate=pl.CostEstimate(flops=flops, bytes_accessed=40000000, transcendentals=0),
-    )(raw_r, raw_o, route, gain, wg, wu, wd, op, outs, fq, ends)
+    )(raw_r, raw_o, ids, scale, decay, gain, wg, wu, wd, op, outs, query)
+
+
+def tail_kernel(
+    gate_in,
+    up_in,
+    down_in,
+    col_hbm,
+    hg_hbm,
+    outs_hbm,
+    fq_hbm,
+    ends_hbm,
+    query_hbm,
+    key_hbm,
+    value_hbm,
+    entry_hbm,
+    decay_ref,
+    gate_out,
+    up_out,
+    down_out,
+    proj_out,
+    query_out,
+    key_out,
+    value_out,
+    gate,
+    up,
+    down,
+    col,
+    hga,
+    outs,
+    fqa,
+    ends,
+    query,
+    key,
+    value,
+    entry,
+    proj,
+    query_grad,
+    key_grad,
+    value_grad,
+    load_sems,
+    store_sems,
+):
+    segs, count, quarter = col.shape
+    heads_here = decay_ref.shape[0]
+    head_width = query.shape[1] // heads_here
+    channels = query.shape[1]
+    loads = []
+
+    def load(src, dst):
+        copy = pltpu.make_async_copy(src, dst, load_sems.at[len(loads)])
+        copy.start()
+        loads.append(copy)
+        return copy
+
+    stores = []
+
+    def store(src, dst):
+        copy = pltpu.make_async_copy(src, dst, store_sems.at[len(stores)])
+        copy.start()
+        stores.append(copy)
+
+    early = [
+        load(*pair)
+        for pair in (
+            (query_hbm, query),
+            (key_hbm, key),
+            (value_hbm, value),
+            (hg_hbm, hga),
+            (fq_hbm, fqa),
+            (ends_hbm, ends),
+            (entry_hbm, entry),
+        )
+    ]
+    load_col = [load(col_hbm, col), load(outs_hbm, outs)]
+    through = [
+        (load(gate_in, gate), gate, gate_out),
+        (load(up_in, up), up, up_out),
+        (load(down_in, down), down, down_out),
+    ]
+    g = lax.axis_index("sp")
+    gy_, gx_ = g // 2, g % 2
+    seg_of = [
+        g,
+        (1 - gy_) * 2 + (1 - gx_),
+        gy_ * 2 + (1 - gx_),
+        (1 - gy_) * 2 + gx_,
+    ]
+    row = lax.broadcasted_iota(jnp.int32, (count, count), 0)
+    column = lax.broadcasted_iota(jnp.int32, (count, count), 1)
+    causal = row >= column
+    decay = decay_ref[...]
+    exact = dict(preferred_element_type=jnp.float32, precision=lax.Precision.HIGHEST)
+    lower = causal.astype(jnp.float32)
+    running = lax.dot_general(lower, decay, (((1,), (1,)), ((), ())), **exact)
+    across = lax.dot_general(decay, lower, (((1,), (1,)), ((), ())), **exact)
+    key_scale = head_width ** (-0.5)
+    bf16 = jnp.bfloat16
+    for copy in early:
+        copy.wait()
+
+    def mul(left, right):
+        return jnp.dot(left, right, preferred_element_type=jnp.float32)
+
+    for h in range(heads_here):
+        cols = slice(h * head_width, (h + 1) * head_width)
+        run = running[:, h : h + 1]
+        from_start = jnp.exp(run)
+        to_end = jnp.exp(running[count - 1 :, h : h + 1] - run)
+        spread = jnp.where(causal, run - across[h : h + 1, :], 0.0)
+        weights = jnp.where(causal, jnp.exp(spread), 0.0)
+        state = jnp.zeros((head_width, head_width), jnp.float32)
+        for j in range(1, segs):
+            between = jnp.zeros((1, 1), jnp.float32)
+            for i in range(1, segs):
+                if i != j:
+                    inside = (seg_of[i] > g) & (seg_of[i] < seg_of[j])
+                    between = between + jnp.where(inside, ends[i, 0:1, h : h + 1], 0.0)
+            passed = jnp.where(seg_of[j] > g, jnp.exp(between), 0.0)
+            state = state + passed * contract_rows(fqa[j, :, cols], hga[j, :, cols])
+        state = state.astype(bf16)
+        grad = hga[0, :, cols]
+        q, k, v = query[:, cols], key[:, cols], value[:, cols]
+        grad_scores = (contract_cols(grad, v) * weights).astype(bf16)
+        key_scores = (contract_cols(q, k) * weights).astype(bf16)
+        query_grad[:, cols] = (
+            key_scale
+            * (mul(grad_scores, k) + from_start * contract_cols(grad, entry[h].astype(bf16)))
+        ).astype(bf16)
+        key_grad[:, cols] = (
+            key_scale * (contract_rows(grad_scores, q) + to_end * contract_cols(v, state))
+        ).astype(bf16)
+        value_grad[:, cols] = (
+            key_scale * (contract_rows(key_scores, grad) + to_end * mul(k, state))
+        ).astype(bf16)
+    store(query_grad, query_out)
+    store(key_grad, key_out)
+    store(value_grad, value_out)
+    for copy, src, dst in through:
+        copy.wait()
+        store(src, dst)
+    for copy in load_col:
+        copy.wait()
+    right = outs[...].reshape(segs * count, channels)
+    for n in range(quarter // 256):
+        cols = slice(n * 256, (n + 1) * 256)
+        proj[cols, :] = contract_rows(col[:, :, cols].reshape(segs * count, 256), right)
+        store(proj.at[cols, :], proj_out.at[cols, :])
+    for copy in stores:
+        copy.wait()
+
+
+def tail_call(gate, up, down, col, hga, outs, fqa, ends, query, key, value, entry, decay):
+    segs, count, quarter = col.shape
+    channels = query.shape[1]
+    any_spec = pl.BlockSpec(memory_space=pl.ANY)
+    shape = jax.ShapeDtypeStruct
+    rows = shape((count, channels), jnp.bfloat16)
+    proj = shape((quarter, channels), jnp.float32)
+    kept = [gate, up, down, col, hga, outs, fqa, ends, query, key, value, entry]
+    results = [proj, rows, rows, rows]
+    return pl.pallas_call(
+        tail_kernel,
+        out_shape=tuple(shape(a.shape, a.dtype) for a in (gate, up, down)) + tuple(results),
+        in_specs=[any_spec] * len(kept) + [pl.BlockSpec(memory_space=pltpu.VMEM)],
+        out_specs=(any_spec,) * 7,
+        scratch_shapes=[pltpu.VMEM(a.shape, a.dtype) for a in kept + results]
+        + [pltpu.SemaphoreType.DMA((12,)), pltpu.SemaphoreType.DMA((16,))],
+        compiler_params=pltpu.CompilerParams(vmem_limit_bytes=VMEM_LIMIT),
+        cost_estimate=pl.CostEstimate(
+            flops=2 * segs * count * quarter * channels,
+            bytes_accessed=30000000,
+            transcendentals=0,
+        ),
+    )(*kept, decay)
 
 
 def local_square(
@@ -699,94 +1019,46 @@
     log_decay,
     entry_state,
 ):
-    token_count, width = residual_mid.shape
+    width = residual_mid.shape[1]
     segs = lax.axis_size("sp")
-    seg = lax.axis_index("sp")
-    heads_here = log_decay.shape[1]
-    experts = jnp.arange(128, dtype=jnp.int32)
-    route = jnp.sum(
-        jnp.where(
-            expert_ids[:, :, None] == experts[None, None, :], expert_weights[:, :, None], 0.0
-        ),
-        axis=1,
-    )
-
-    def split_heads(rows):
-        return rows.reshape(token_count, heads_here, -1).transpose(1, 0, 2)
-
-    running = jnp.cumsum(log_decay, axis=0).T
-    from_start = jnp.exp(running)
-    head_width = query_rows.shape[1] // heads_here
-    fq = (
-        jnp.repeat(from_start.T, head_width, axis=1) * query_rows.astype(jnp.float32)
-    ).astype(jnp.bfloat16)
-    ends = jnp.zeros((8, 128), jnp.float32).at[:, :heads_here].set(running[:, -1][None, :])
-    gate_grad, up_grad, down_grad, columns, grads, outs, fqs, ends_all = square_call(
+    gate_grad, up_grad, down_grad, columns, grads, outs, fqs, ends = square_call(
         segs,
         residual_mid,
         out_grad,
-        route,
+        expert_ids.T,
+        expert_weights.T,
+        log_decay.T,
         norm_gain.reshape(1, width),
         gate_proj[0],
         up_proj[0],
         down_proj[0],
         out_proj,
         retention_out,
-        fq,
+        query_rows,
+    )
+    gate_grad, up_grad, down_grad, proj_grad, query_grad, key_grad, value_grad = tail_call(
+        gate_grad,
+        up_grad,
+        down_grad,
+        columns,
+        grads,
+        outs,
+        fqs,
         ends,
-    )
-    proj_grad = contract_rows(
-        columns.reshape(segs * token_count, -1), outs.reshape(segs * token_count, -1)
-    )
-    seg_decay = ends_all[:, 0, :heads_here]
-    head_grad = lax.dynamic_index_in_dim(grads, seg, axis=0, keepdims=False)
-    queries = split_heads(query_rows)
-    key_heads = split_heads(key_rows)
-    value_heads = split_heads(value_rows)
-    grad_heads = split_heads(head_grad)
-    key_scale = queries.shape[2] ** (-0.5)
-    to_end = jnp.exp(running[:, -1:] - running)
-    position = jnp.arange(token_count, dtype=jnp.int32)
-    causal = (position[:, None] >= position[None, :])[None]
-    spread = jnp.where(causal, running[:, :, None] - running[:, None, :], 0.0)
-    weights = jnp.where(causal, jnp.exp(spread), 0.0)
-    states = dots(
-        "gthk,gthe->ghke",
-        fqs.reshape(segs, token_count, heads_here, head_width),
-        grads.reshape(segs, token_count, heads_here, head_width),
-    )
-    order = jnp.arange(segs, dtype=jnp.int32)
-    between = (order[None, :] > seg) & (order[None, :] < order[:, None])
-    passed = jnp.exp(jnp.sum(jnp.where(between[:, :, None], seg_decay[None], 0.0), axis=1))
-    passed = jnp.where(order[:, None] > seg, passed, 0.0)
-    later_state = jnp.sum(passed[:, :, None, None] * states, axis=0)
-    entry = entry_state[0]
-    grad_scores = dots("hte,hse->hts", grad_heads, value_heads) * weights
-    key_scores = dots("htk,hsk->hts", queries, key_heads) * weights
-    query_grad = key_scale * (
-        dots("hts,hsk->htk", grad_scores, key_heads)
-        + from_start[:, :, None] * dots("hte,hke->htk", grad_heads, entry)
-    )
-    key_grad = key_scale * (
-        dots("hts,htk->hsk", grad_scores, queries)
-        + to_end[:, :, None] * dots("hse,hke->hsk", value_heads, later_state)
-    )
-    value_grad = key_scale * (
-        dots("hts,hte->hse", key_scores, grad_heads)
-        + to_end[:, :, None] * dots("hsk,hke->hse", key_heads, later_state)
-    )
-
-    def merge_heads(heads_rows):
-        return heads_rows.transpose(1, 0, 2).reshape(token_count, -1).astype(jnp.bfloat16)
-
+        query_rows,
+        key_rows,
+        value_rows,
+        entry_state[0],
+        log_decay.T,
+    )
     return (
         gate_grad[None],
         up_grad[None],
         down_grad[None],
         proj_grad,
-        merge_heads(query_grad),
-        merge_heads(key_grad),
-        merge_heads(value_grad),
+        query_grad,
+        key_grad,
+        value_grad,
     )
 
 

time: 151 us -> 121 us (0.80)
  local copies, waits for them, and re-layouts: 12.1 us -> 0 us
  Pallas kernels: 126 us -> 119 us
  matrix products: 6 us -> 0 us
  other arithmetic: 5.46 us -> 0 us
    pallas_call x1, Pallas kernels: 126 us -> 110 us  [square_call(): pl.pallas_call(square_kernel, out_shape=(shape((width, feats), bf16), sha...]
    pallas_call x0 -> x1, Pallas kernels: none -> 8.19 us  [tail_call(): pl.pallas_call(tail_kernel, out_shape=tuple((shape(a.shape, a.dtype) for...]
    unnamed x24 -> x0, local copies, waits for them, and re-layouts: 6.2 us -> none
    dot_general x9 -> x0, matrix products: 6 us -> none  [the longest x8 3.67 us: dots(): jnp.einsum(spec, left.astype(jnp.bfloat16), right.astype(jnp.bfloat16), p...]
    another operation x4 -> x0, other arithmetic: 2.07 us -> none
    convert_element_type x3 -> x0, local copies, waits for them, and re-layouts: 2.04 us -> none  [merge_heads(): heads_rows.transpose(1, 0, 2).reshape(token_count, -1).astype(jnp.bfloat16)]
    convert_element_type x1 -> x0, other arithmetic: 1.62 us -> none  [local_square(): fq = (jnp.repeat(from_start.T, head_width, axis=1) * query_rows.astype(jn...]
    reduce_sum x2 -> x0, other arithmetic: 1.58 us -> none  [the longest x1 1.49 us: local_square(): jnp.sum(jnp.where(expert_ids[:, :, None] == experts[None, None, :], exper...]
where the time goes in v2:
time: 121 us; the launch traced here: 119 us
  Pallas kernels  119 us (98%)
    pallas_call x1, Pallas kernels, square_call(): pl.pallas_call(square_kernel, out_shape=(shape((width, feats), bf16), sha...  110 us
    pallas_call x1, Pallas kernels, tail_call(): pl.pallas_call(tail_kernel, out_shape=tuple((shape(a.shape, a.dtype) for...  8.19 us

profile of v2, /device:TPU:27, one launch (start us, length us, event | category | flops | bytes accessed | tf_op | source)
XLA Modules:
  0.0 119.4 jit_solution(14428321651429464840)
XLA Ops:
  0.6 110.4 %shard_map.198 = (bf16[4096,256]{1,0:T(8,128)(2,1)}, bf16[4096,256]{1,0:T(8,128)(2,1)}, bf16[256,4096]{1,0:T(8,128)(2,1)}, bf16[4,160,1024]{2,1,0:T(8,128)(2,1)}...) custom-call(bf16[160,4096]{1,0:T(8,128)(2,1)} %raw_r_hbm.1, ...), custom_call_target="tpu_custom_call" | custom-call | flops 10737418240 | bytes 40000000 | tf_op jit(solution)/shard_map/pallas_call | solution.py:765
  111.1 8.2 %shard_map.199 = (bf16[4096,256]{1,0:T(8,128)(2,1)}, bf16[4096,256]{1,0:T(8,128)(2,1)}, bf16[256,4096]{1,0:T(8,128)(2,1)}, f32[1024,512]{1,0:T(8,128)}, bf16[160...) custom-call(bf16[4096,256]{1,0:T(8,128)(2,1)} %get-tuple-element.22.gate_in, ...), custom_call_target="tpu_custom_call" | custom-call | flops 671088640 | bytes 30000000 | tf_op jit(solution)/shard_map/pallas_call | solution.py:989

commit v3 on v2

--- a/solution.py
+++ b/solution.py
@@ -222,10 +222,10 @@
 def square_kernel(
     raw_r_hbm,
     raw_o_hbm,
-    ids_ref,
-    scale_ref,
-    decay_ref,
-    gain_ref,
+    ids_hbm,
+    scale_hbm,
+    decay_hbm,
+    gain_hbm,
     wg_hbm,
     wu_hbm,
     wd_hbm,
@@ -240,6 +240,10 @@
     outs_out,
     fq_out,
     ends_out,
+    ids_ref,
+    scale_ref,
+    decay_ref,
+    gain_ref,
     raw_r,
     raw_o,
     rin,
@@ -248,6 +252,8 @@
     wg,
     wu,
     wd,
+    wdt,
+    wgut,
     op,
     part,
     pin,
@@ -255,6 +261,7 @@
     back,
     pre,
     hgrad,
+    slope_m,
     query,
     rx,
     ry,
@@ -347,8 +354,11 @@
         copy.start()
         stores.append(copy)
 
+    load_small = [load(ids_hbm, ids_ref), load(scale_hbm, scale_ref)]
+    load_gain = load(gain_hbm, gain_ref)
     load_r = load(raw_r_hbm, raw_r)
     load_o = load(raw_o_hbm, raw_o)
+    load_decay = load(decay_hbm, decay_ref)
     load_w = [load(wg_hbm, wg), load(wu_hbm, wu), load(wd_hbm, wd)]
     load_op = load(op_hbm, op)
     load_outs = load(outs_hbm, outs_all.at[0])
@@ -363,6 +373,8 @@
 
     kinds = (g, gd, gx, gy)
     which = lax.broadcasted_iota(jnp.int32, (8, count), 0)
+    for copy in load_small:
+        copy.wait()
     table = jnp.zeros((8, count), jnp.float32)
     for k, expert in enumerate(kinds):
         chosen = jnp.where(ids_ref[...] == expert, scale_ref[...], 0.0)
@@ -404,6 +416,7 @@
 
         lax.fori_loop(0, rows // ROWS, step, 0)
 
+    load_gain.wait()
     load_r.wait()
     normalize(c * half, half)
     pl.semaphore_wait(barrier, 4 + len(along))
@@ -414,9 +427,18 @@
     x_n = put(rin.at[0, mine, :], rin.at[2, mine, :], X)
     y_n = put(rin.at[0, mine, :], rin.at[3, mine, :], Y)
     weigh(c * half, half, 2, stage(0))
-    x_o = put(stg.at[0], og.at[2, mine, :], X)
+    line_rows = rz1.shape[1]
+    cuts = [(0, line_rows), (line_rows, half - line_rows)]
+
+    def rows_of(cut):
+        return pl.ds(pl.multiple_of(c * half + cut[0], ROWS), cut[1])
+
+    def send_cut(index, slot, target, cut):
+        return put(stg.at[index, slice(cut[0], cut[0] + cut[1]), :], og.at[slot, rows_of(cut), :], target)
+
+    x_o = [send_cut(0, 2, X, cut) for cut in cuts]
     weigh(c * half, half, 3, stage(1))
-    y_o = put(stg.at[1], og.at[3, mine, :], Y)
+    y_o = [send_cut(1, 3, Y, cut) for cut in cuts]
 
     def spread(buf):
         block = buf.at[1, mine, span(z)]
@@ -438,6 +460,7 @@
     d_o.wait_recv()
     o_spread = spread(og)
 
+    load_decay.wait()
     heads_here = decay_ref.shape[0]
     head_width = query.shape[1] // heads_here
     later = lax.broadcasted_iota(jnp.int32, (count, count), 0)
@@ -469,27 +492,25 @@
             lhs, wu[...], preferred_element_type=jnp.float32
         ).reshape(-1, count, feats)
 
-    def hidden_grads(slots, rows):
-        lhs = og[slots].reshape(rows, width)
-        hgrad[slots] = contract_cols(lhs, wd[...]).reshape(-1, count, feats)
-
-    def activations(s):
-        hidden, pullback = jax.vjp(activate, pre[s, :, :feats], pre[s, :, feats:])
-        gate_back, up_back = pullback(hgrad[s])
-        both = gate_back * pre[s, :, :feats] + up_back * pre[s, :, feats:]
+    def slopes(s):
+        gate_pre, up_pre = pre[s, :, :feats], pre[s, :, feats:]
+        hidden, pullback = jax.vjp(activate, gate_pre, up_pre)
+        gate_slope, up_slope = pullback(jnp.ones_like(hidden))
+        hid[s] = hidden.astype(jnp.bfloat16)
+        slope_m[s] = gate_slope * gate_pre + up_slope * up_pre
+        pre[s, :, :feats] = gate_slope
+        pre[s, :, feats:] = up_slope
+
+    def backward(s):
+        grad = hgrad[s]
         mrow[0, s] = lax.dot_general(
-            jnp.ones((8, feats), jnp.float32), both, (((1,), (1,)), ((), ())), **exact
+            jnp.ones((8, feats), jnp.float32),
+            grad * slope_m[s],
+            (((1,), (1,)), ((), ())),
+            **exact,
         )
-        hid[s] = hidden.astype(jnp.bfloat16)
-        back[s, :, :feats] = gate_back.astype(jnp.bfloat16)
-        back[s, :, feats:] = up_back.astype(jnp.bfloat16)
-
-    def part_step(slots, rows, cols):
-        lhs = back[slots].reshape(rows, 2 * feats)
-        piece = contract_cols(lhs[:, :feats], wg[cols, :]) + contract_cols(
-            lhs[:, feats:], wu[cols, :]
-        )
-        part[slots, :, cols] = piece.astype(jnp.bfloat16).reshape(-1, count, quarter)
+        back[s, :, :feats] = (grad * pre[s, :, :feats]).astype(jnp.bfloat16)
+        back[s, :, feats:] = (grad * pre[s, :, feats:]).astype(jnp.bfloat16)
 
     def pair_step(s, cols):
         def step(i, carry):
@@ -502,16 +523,30 @@
         lax.fori_loop(0, half // ROWS, step, 0)
 
     gates(slice(0, 1), count)
-    hidden_grads(slice(0, 1), count)
-    activations(0)
+    slopes(0)
+    hgrad[0] = contract_cols(og[0], wd[...])
+    backward(0)
 
     def own_step(n, carry):
-        part_step(slice(0, 1), count, span(n))
+        cols = span(n)
+        piece = contract_cols(back[0, :, :feats], wg[cols, :]) + contract_cols(
+            back[0, :, feats:], wu[cols, :]
+        )
+        part[0, :, cols] = piece.astype(jnp.bfloat16)
         return carry
 
     lax.fori_loop(0, depth, own_step, 0)
     swap_own = put(part.at[0, theirs, :], pin.at[0], across)
 
+
+    def turn(n, carry):
+        cols = pl.ds(pl.multiple_of(n * 512, 128), 512)
+        wdt[cols, :] = wd[:, cols].T
+        wgut[:feats, cols] = wg[cols, :].T
+        wgut[feats:, cols] = wu[cols, :].T
+        return carry
+
+    lax.fori_loop(0, width // 512, turn, 0)
     rest = (segs - 1) * count
     x_n.wait_recv()
     f = [forward(rin, 2)]
@@ -523,13 +558,16 @@
     for copy in f:
         copy.wait_recv()
     gates(slice(1, segs), rest)
+    for slot in range(1, segs):
+        slopes(slot)
     f = []
     for i in range(depth - 1):
         f.append(collect(og, o_spread, i))
-    x_o.wait_recv()
-    f.append(forward(og, 2))
-    y_o.wait_recv()
-    f.append(forward(og, 3))
+    for k, cut in enumerate(cuts):
+        for slot, copies in ((2, x_o), (3, y_o)):
+            copies[k].wait_recv()
+            block = og.at[slot, rows_of(cut), :]
+            f.append(put(block, block, across))
     o_spread[-1].wait_recv()
     for copy in f:
         copy.wait_recv()
@@ -548,7 +586,6 @@
 
         lax.fori_loop(0, half // ROWS, step, 0)
 
-    line_rows = rz1.shape[1]
     on_line = pl.ds(pl.multiple_of(c * half, ROWS), line_rows)
     direct = pl.ds(pl.multiple_of(c * half + line_rows, ROWS), half - line_rows)
     order = [span(q) for q in ups] + [span(z)]
@@ -567,12 +604,30 @@
         if n < depth - 1:
             d_z.append(put(part.at[1, on_line, cols], rz1.at[n], along[n]))
 
-    hidden_grads(slice(1, segs), rest)
+    halves = [
+        jnp.dot(
+            jnp.concatenate([og[1, part_rows], og[2, part_rows], og[3, part_rows]], axis=0),
+            wdt[...],
+            preferred_element_type=jnp.float32,
+        )
+        for part_rows in (slice(0, half), slice(half, count))
+    ]
     for slot in range(1, segs):
-        activations(slot)
+        for k, part_rows in enumerate((slice(0, half), slice(half, count))):
+            hgrad[slot, part_rows] = halves[k][(slot - 1) * half : slot * half]
+    for slot in range(1, segs):
+        backward(slot)
     m_pair = put(mrow.at[0], mrow.at[1], across)
     for n, cols in enumerate(order):
-        part_step(slice(1, segs), rest, cols)
+        part[1:, :, cols] = (
+            jnp.dot(
+                back[1:].reshape(rest, 2 * feats),
+                wgut[:, cols],
+                preferred_element_type=jnp.float32,
+            )
+            .astype(jnp.bfloat16)
+            .reshape(segs - 1, count, quarter)
+        )
         swaps.append(
             [
                 put(part.at[slot, theirs, cols], pin.at[slot, :, cols], across)
@@ -619,8 +674,6 @@
                 copy.wait_recv()
             lax.fori_loop(0, line_rows // ROWS, line_step, 0)
             d_p = put(sd, rd, Z)
-            for slot, target in ((1, Z), (2, X), (3, Y)):
-                extras.append(put(outs_all.at[0], outs_all.at[slot], target))
         for copies in (x_p, y_p, dd_p):
             copies[n].wait_recv()
 
@@ -655,17 +708,6 @@
             m_z = [put(msend, mz.at[i], along[i]) for i in range(depth - 1)]
         if n < depth - 1:
             own_z.append(put(part.at[0, mine, cols], rz2.at[n], along[n]))
-
-    def down_step(n, carry):
-        cols = pl.ds(pl.multiple_of(n * 512, 128), 512)
-        block = contract_rows(
-            hid[...].reshape(segs * count, feats), og[:, :, cols].reshape(segs * count, 512)
-        )
-        dout[:, cols] = block.astype(jnp.bfloat16)
-        return carry
-
-    lax.fori_loop(0, width // 512, down_step, 0)
-    store(dout, down_out)
 
     d_p.wait_recv()
 
@@ -694,47 +736,77 @@
         grad = raw_o[r, span(z)].astype(jnp.float32) + inverse * (weighted - scaled * means[r, 0:1])
         rg[r, span(z)] = grad.astype(jnp.bfloat16)
 
-    def resid_line(i, carry):
-        resid_step(i, True)
-        return carry
-
-    def resid_direct(i, carry):
-        resid_step(i, None)
-        return carry
-
-    lax.fori_loop(0, line_rows // ROWS, resid_line, 0)
-    lax.fori_loop(line_rows // ROWS, half // ROWS, resid_direct, 0)
-    block = rg.at[mine, span(z)]
-    g_z = line_put(block)
-    g_f = [put(block, block, across)]
-    col_copies = [
-        (t, slot, remote(rg.at[mine, span(t)], col.at[slot, mine, :], target))
-        for t, slot, target in ((gd, 1, Z), (gx, 2, X), (gy, 3, Y))
-    ]
-
-    def send_columns(q):
-        for t, _, copy in col_copies:
+    pieces = [(0, line_rows, True), (line_rows, half - line_rows, None)]
+    g_z, g_f, col_copies = [], [], []
+
+    def send_columns(k, q):
+        for t, _, copy in col_copies[k]:
 
             @pl.when(q == t)
             def _():
                 copy.start()
 
-    send_columns(z)
-    for i in range(depth - 1):
-        g_z[i].wait_recv()
-        block = rg.at[mine, span(downs[i])]
-        g_f.append(put(block, block, across))
-        send_columns(downs[i])
-    for copy in g_f:
-        copy.wait_recv()
+    def resid_piece(k):
+        first_row, size, extra = pieces[k]
+
+        def resid_loop(i, carry):
+            resid_step(i, extra)
+            return carry
+
+        lax.fori_loop(first_row // ROWS, (first_row + size) // ROWS, resid_loop, 0)
+        rows = pl.ds(pl.multiple_of(c * half + first_row, ROWS), size)
+        block = rg.at[rows, span(z)]
+        g_z.append(line_put(block))
+        g_f.append([put(block, block, across)])
+        col_copies.append(
+            [
+                (t, slot, remote(rg.at[rows, span(t)], col.at[slot, rows, :], target))
+                for t, slot, target in ((gd, 1, Z), (gx, 2, X), (gy, 3, Y))
+            ]
+        )
+        send_columns(k, z)
+
+    resid_piece(0)
+    def down_step(n, carry):
+        cols = pl.ds(pl.multiple_of(n * 512, 128), 512)
+        block = contract_rows(
+            hid[...].reshape(segs * count, feats), og[:, :, cols].reshape(segs * count, 512)
+        )
+        dout[:, cols] = block.astype(jnp.bfloat16)
+        return carry
+
+    lax.fori_loop(0, width // 512, down_step, 0)
+    store(dout, down_out)
+
+    resid_piece(1)
+    for slot, target in ((1, Z), (2, X), (3, Y)):
+        extras.append(put(outs_all.at[0], outs_all.at[slot], target))
     load_op.wait()
-    hga[0] = contract_cols(rg[...], op[...]).astype(jnp.bfloat16)
-    heads = [put(hga.at[0], hga.at[slot], t) for slot, t in ((1, Z), (2, X), (3, Y))]
+    heads, col_f = [], []
+    for k, (first_row, size, extra) in enumerate(pieces):
+        rows = pl.ds(pl.multiple_of(c * half + first_row, ROWS), size)
+        for i in range(depth - 1):
+            g_z[k][i].wait_recv()
+            block = rg.at[rows, span(downs[i])]
+            g_f[k].append(put(block, block, across))
+            send_columns(k, downs[i])
+        for copy in g_f[k]:
+            copy.wait_recv()
+        spots = [slice(base + first_row, base + first_row + size) for base in (0, half)]
+        lhs = jnp.concatenate([rg[spot, :] for spot in spots], axis=0)
+        grads = contract_cols(lhs, op[...]).astype(jnp.bfloat16)
+        for j, spot in enumerate(spots):
+            hga[0, spot, :] = grads[j * size : (j + 1) * size]
+        for spot in spots:
+            for slot, target in ((1, Z), (2, X), (3, Y)):
+                heads.append(put(hga.at[0, spot], hga.at[slot, spot], target))
     col[0] = rg[:, span(g)]
-    col_f = []
-    for _, slot, copy in col_copies:
-        copy.wait_recv()
-        col_f.append(forward(col, slot))
+    for k, (first_row, size, extra) in enumerate(pieces):
+        rows = pl.ds(pl.multiple_of(c * half + first_row, ROWS), size)
+        for _, slot, copy in col_copies[k]:
+            copy.wait_recv()
+            block = col.at[slot, rows, :]
+            col_f.append(put(block, block, across))
     for copy in extras:
         copy.wait_recv()
     store(outs_all, outs_out)
@@ -759,7 +831,6 @@
     line = half * 3 // 5 // ROWS * ROWS
     bf16, f32 = jnp.bfloat16, jnp.float32
     any_spec = pl.BlockSpec(memory_space=pl.ANY)
-    vmem_spec = pl.BlockSpec(memory_space=pltpu.VMEM)
     shape = jax.ShapeDtypeStruct
     flops = 2 * segs * count * width * feats * 8
     return pl.pallas_call(
@@ -774,9 +845,13 @@
             shape((segs, count, heads), bf16),
             shape((segs, 8, 128), f32),
         ),
-        in_specs=[any_spec] * 2 + [vmem_spec] * 4 + [any_spec] * 6,
+        in_specs=[any_spec] * 12,
         out_specs=(any_spec,) * 8,
         scratch_shapes=[
+            pltpu.VMEM(ids.shape, jnp.int32),
+            pltpu.VMEM(scale.shape, f32),
+            pltpu.VMEM(decay.shape, f32),
+            pltpu.VMEM(gain.shape, f32),
             pltpu.VMEM((count, width), bf16),
             pltpu.VMEM((count, width), bf16),
             pltpu.VMEM((segs, count, width), bf16),
@@ -785,12 +860,15 @@
             pltpu.VMEM((width, feats), bf16),
             pltpu.VMEM((width, feats), bf16),
             pltpu.VMEM((feats, width), bf16),
+            pltpu.VMEM((width, feats), bf16),
+            pltpu.VMEM((2 * feats, width), bf16),
             pltpu.VMEM((heads, width), bf16),
             pltpu.VMEM((segs, count, width), bf16),
             pltpu.VMEM((segs, half, width), bf16),
             pltpu.VMEM((segs, count, feats), bf16),
             pltpu.VMEM((segs, count, 2 * feats), bf16),
             pltpu.VMEM((segs, count, 2 * feats), f32),
+            pltpu.VMEM((segs, count, feats), f32),
             pltpu.VMEM((segs, count, feats), f32),
             pltpu.VMEM((count, heads), bf16),
             pltpu.VMEM((half, width), bf16),
@@ -816,9 +894,9 @@
             pltpu.VMEM((width, feats), bf16),
             pltpu.VMEM((width, feats), bf16),
             pltpu.VMEM((feats, width), bf16),
-            pltpu.SemaphoreType.DMA((96,)),
-            pltpu.SemaphoreType.DMA((96,)),
-            pltpu.SemaphoreType.DMA((8,)),
+            pltpu.SemaphoreType.DMA((160,)),
+            pltpu.SemaphoreType.DMA((160,)),
+            pltpu.SemaphoreType.DMA((12,)),
             pltpu.SemaphoreType.DMA((8,)),
         ],
         compiler_params=pltpu.CompilerParams(
@@ -841,7 +919,7 @@
     key_hbm,
     value_hbm,
     entry_hbm,
-    decay_ref,
+    decay_hbm,
     gate_out,
     up_out,
     down_out,
@@ -861,6 +939,7 @@
     key,
     value,
     entry,
+    decay_ref,
     proj,
     query_grad,
     key_grad,
@@ -890,6 +969,7 @@
     early = [
         load(*pair)
         for pair in (
+            (decay_hbm, decay_ref),
             (query_hbm, query),
             (key_hbm, key),
             (value_hbm, value),
@@ -916,6 +996,7 @@
     row = lax.broadcasted_iota(jnp.int32, (count, count), 0)
     column = lax.broadcasted_iota(jnp.int32, (count, count), 1)
     causal = row >= column
+    early[0].wait()
     decay = decay_ref[...]
     exact = dict(preferred_element_type=jnp.float32, precision=lax.Precision.HIGHEST)
     lower = causal.astype(jnp.float32)
@@ -923,7 +1004,7 @@
     across = lax.dot_general(decay, lower, (((1,), (1,)), ((), ())), **exact)
     key_scale = head_width ** (-0.5)
     bf16 = jnp.bfloat16
-    for copy in early:
+    for copy in early[1:]:
         copy.wait()
 
     def mul(left, right):
@@ -984,22 +1065,22 @@
     shape = jax.ShapeDtypeStruct
     rows = shape((count, channels), jnp.bfloat16)
     proj = shape((quarter, channels), jnp.float32)
-    kept = [gate, up, down, col, hga, outs, fqa, ends, query, key, value, entry]
+    kept = [gate, up, down, col, hga, outs, fqa, ends, query, key, value, entry, decay]
     results = [proj, rows, rows, rows]
     return pl.pallas_call(
         tail_kernel,
         out_shape=tuple(shape(a.shape, a.dtype) for a in (gate, up, down)) + tuple(results),
-        in_specs=[any_spec] * len(kept) + [pl.BlockSpec(memory_space=pltpu.VMEM)],
+        in_specs=[any_spec] * len(kept),
         out_specs=(any_spec,) * 7,
         scratch_shapes=[pltpu.VMEM(a.shape, a.dtype) for a in kept + results]
-        + [pltpu.SemaphoreType.DMA((12,)), pltpu.SemaphoreType.DMA((16,))],
+        + [pltpu.SemaphoreType.DMA((16,)), pltpu.SemaphoreType.DMA((16,))],
         compiler_params=pltpu.CompilerParams(vmem_limit_bytes=VMEM_LIMIT),
         cost_estimate=pl.CostEstimate(
             flops=2 * segs * count * quarter * channels,
             bytes_accessed=30000000,
             transcendentals=0,
         ),
-    )(*kept, decay)
+    )(*kept)
 
 
 def local_square(

time: 121 us -> 113 us (0.934); the launches traced: 119 us -> 113 us
  Pallas kernels: 119 us -> 112 us
    pallas_call x1, Pallas kernels: 110 us -> 105 us  [square_call(): pl.pallas_call(square_kernel, out_shape=(shape((width, feats), bf16), sha...]
where the time goes in v3:
time: 113 us
  Pallas kernels  112 us (99%)
    pallas_call x1, Pallas kernels, square_call(): pl.pallas_call(square_kernel, out_shape=(shape((width, feats), bf16), sha...  105 us
    pallas_call x1, Pallas kernels, tail_call(): pl.pallas_call(tail_kernel, out_shape=tuple((shape(a.shape, a.dtype) for...  7.54 us

profile of v3, /device:TPU:27, one launch (start us, length us, event | category | flops | bytes accessed | tf_op | source)
XLA Modules:
  0.0 113.1 jit_solution(4026673255648915181)
XLA Ops:
  0.6 104.8 %shard_map.198 = (bf16[4096,256]{1,0:T(8,128)(2,1)}, bf16[4096,256]{1,0:T(8,128)(2,1)}, bf16[256,4096]{1,0:T(8,128)(2,1)}, bf16[4,160,1024]{2,1,0:T(8,128)(2,1)}...) custom-call(bf16[160,4096]{1,0:T(8,128)(2,1)} %raw_r_hbm.1, ...), custom_call_target="tpu_custom_call" | custom-call | flops 10737418240 | bytes 40000000 | tf_op jit(solution)/shard_map/pallas_call | solution.py:836
  105.4 7.5 %shard_map.199 = (bf16[4096,256]{1,0:T(8,128)(2,1)}, bf16[4096,256]{1,0:T(8,128)(2,1)}, bf16[256,4096]{1,0:T(8,128)(2,1)}, f32[1024,512]{1,0:T(8,128)}, bf16[160...) custom-call(bf16[4096,256]{1,0:T(8,128)(2,1)} %get-tuple-element.22.gate_in, ...), custom_call_target="tpu_custom_call" | custom-call | flops 671088640 | bytes 30000000 | tf_op jit(solution)/shard_map/pallas_call | solution.py:1070

commit v4 on v3

--- a/solution.py
+++ b/solution.py
@@ -215,6 +215,7 @@
 
 
 ROWS = 16
+COPIES = 117
 VMEM_LIMIT = 66 * 1000 * 1000
 MESH_ID = pl.DeviceIdType.MESH
 
@@ -476,9 +477,9 @@
     ends_all[0, :, :heads_here] = jnp.broadcast_to(running[count - 1 :, :], (8, heads_here))
     load_outs.wait()
     extras = []
-    for slot, target in ((1, Z), (2, X), (3, Y)):
-        for buf in (ends_all, fq_all):
-            extras.append(put(buf.at[0], buf.at[slot], target))
+    for slot, target in ((2, X), (3, Y), (1, Z)):
+        extras.append(put(ends_all.at[0], ends_all.at[slot], target))
+    shared = [put(fq_all.at[0], fq_all.at[slot], target) for slot, target in ((2, X), (3, Y))]
 
     for copy in load_w:
         copy.wait()
@@ -593,8 +594,7 @@
 
     def advance(n):
         cols = order[n]
-        for copy in swaps[n]:
-            copy.wait_recv()
+        swaps[n].wait_recv()
         pair_step(2, cols)
         x_p.append(put(part.at[2, mine, cols], rx.at[:, cols], X))
         pair_step(3, cols)
@@ -628,12 +628,8 @@
             .astype(jnp.bfloat16)
             .reshape(segs - 1, count, quarter)
         )
-        swaps.append(
-            [
-                put(part.at[slot, theirs, cols], pin.at[slot, :, cols], across)
-                for slot in (2, 3, 1)
-            ]
-        )
+        others = pl.ds(1, segs - 1)
+        swaps.append(put(part.at[others, theirs, cols], pin.at[others, :, cols], across))
         if n == 1:
             m_pair.wait_recv()
             mrow[2] = mrow[0] + mrow[1]
@@ -736,7 +732,10 @@
         grad = raw_o[r, span(z)].astype(jnp.float32) + inverse * (weighted - scaled * means[r, 0:1])
         rg[r, span(z)] = grad.astype(jnp.bfloat16)
 
-    pieces = [(0, line_rows, True), (line_rows, half - line_rows, None)]
+    pieces = []
+    while sum(size for _, size in pieces) < half:
+        first_row = sum(size for _, size in pieces)
+        pieces.append((first_row, min(2 * ROWS, half - first_row)))
     g_z, g_f, col_copies = [], [], []
 
     def send_columns(k, q):
@@ -746,14 +745,19 @@
             def _():
                 copy.start()
 
+    def resid_line(i, carry):
+        resid_step(i, True)
+        return carry
+
+    def resid_direct(i, carry):
+        resid_step(i, None)
+        return carry
+
+    lax.fori_loop(0, line_rows // ROWS, resid_line, 0)
+    lax.fori_loop(line_rows // ROWS, half // ROWS, resid_direct, 0)
+
     def resid_piece(k):
-        first_row, size, extra = pieces[k]
-
-        def resid_loop(i, carry):
-            resid_step(i, extra)
-            return carry
-
-        lax.fori_loop(first_row // ROWS, (first_row + size) // ROWS, resid_loop, 0)
+        first_row, size = pieces[k]
         rows = pl.ds(pl.multiple_of(c * half + first_row, ROWS), size)
         block = rg.at[rows, span(z)]
         g_z.append(line_put(block))
@@ -767,6 +771,11 @@
         send_columns(k, z)
 
     resid_piece(0)
+    for slot, target in ((2, X), (3, Y), (1, Z)):
+        extras.append(put(outs_all.at[0], outs_all.at[slot], target))
+    for k, (rows, target) in enumerate(((slice(0, half), Y), (slice(half, count), X))):
+        shared[k].wait_recv()
+        extras.append(put(fq_all.at[2 + k, rows], fq_all.at[1, rows], target))
     def down_step(n, carry):
         cols = pl.ds(pl.multiple_of(n * 512, 128), 512)
         block = contract_rows(
@@ -779,29 +788,40 @@
     store(dout, down_out)
 
     resid_piece(1)
-    for slot, target in ((1, Z), (2, X), (3, Y)):
-        extras.append(put(outs_all.at[0], outs_all.at[slot], target))
     load_op.wait()
+
+    def turn_op(n, carry):
+        cols = pl.ds(pl.multiple_of(n * 512, 128), 512)
+        wg[cols, :] = op[:feats, cols].T
+        wu[cols, :] = op[feats:, cols].T
+        return carry
+
+    lax.fori_loop(0, width // 512, turn_op, 0)
     heads, col_f = [], []
-    for k, (first_row, size, extra) in enumerate(pieces):
+    for k, (first_row, size) in enumerate(pieces):
         rows = pl.ds(pl.multiple_of(c * half + first_row, ROWS), size)
         for i in range(depth - 1):
             g_z[k][i].wait_recv()
             block = rg.at[rows, span(downs[i])]
             g_f[k].append(put(block, block, across))
             send_columns(k, downs[i])
+        if k + 2 < len(pieces):
+            resid_piece(k + 2)
         for copy in g_f[k]:
             copy.wait_recv()
-        spots = [slice(base + first_row, base + first_row + size) for base in (0, half)]
-        lhs = jnp.concatenate([rg[spot, :] for spot in spots], axis=0)
-        grads = contract_cols(lhs, op[...]).astype(jnp.bfloat16)
-        for j, spot in enumerate(spots):
-            hga[0, spot, :] = grads[j * size : (j + 1) * size]
-        for spot in spots:
-            for slot, target in ((1, Z), (2, X), (3, Y)):
-                heads.append(put(hga.at[0, spot], hga.at[slot, spot], target))
+        spot = slice(first_row, first_row + size)
+        lhs = jnp.concatenate(
+            [rg[base + first_row : base + first_row + size, :] for base in (0, half)], axis=0
+        )
+        for k, turned in enumerate((wg, wu)):
+            grads = jnp.dot(lhs, turned[...], preferred_element_type=jnp.float32)
+            grads = grads.astype(jnp.bfloat16)
+            for j in range(CORES):
+                hga[0, j, spot, k * feats : (k + 1) * feats] = grads[j * size : (j + 1) * size]
+        for slot, target in ((1, Z), (2, X), (3, Y)):
+            heads.append(put(hga.at[0, :, spot], hga.at[slot, :, spot], target))
     col[0] = rg[:, span(g)]
-    for k, (first_row, size, extra) in enumerate(pieces):
+    for k, (first_row, size) in enumerate(pieces):
         rows = pl.ds(pl.multiple_of(c * half + first_row, ROWS), size)
         for _, slot, copy in col_copies[k]:
             copy.wait_recv()
@@ -840,7 +860,7 @@
             shape((width, feats), bf16),
             shape((feats, width), bf16),
             shape((segs, count, quarter), bf16),
-            shape((segs, count, heads), bf16),
+            shape((segs, CORES, half, heads), bf16),
             shape((segs, count, heads), bf16),
             shape((segs, count, heads), bf16),
             shape((segs, 8, 128), f32),
@@ -887,15 +907,15 @@
             pltpu.VMEM((segs - 1, 8, count), f32),
             pltpu.VMEM((count, width), bf16),
             pltpu.VMEM((segs, count, quarter), bf16),
-            pltpu.VMEM((segs, count, heads), bf16),
+            pltpu.VMEM((segs, CORES, half, heads), bf16),
             pltpu.VMEM((segs, count, heads), bf16),
             pltpu.VMEM((segs, count, heads), bf16),
             pltpu.VMEM((segs, 8, 128), f32),
             pltpu.VMEM((width, feats), bf16),
             pltpu.VMEM((width, feats), bf16),
             pltpu.VMEM((feats, width), bf16),
-            pltpu.SemaphoreType.DMA((160,)),
-            pltpu.SemaphoreType.DMA((160,)),
+            pltpu.SemaphoreType.DMA((COPIES,)),
+            pltpu.SemaphoreType.DMA((COPIES,)),
             pltpu.SemaphoreType.DMA((12,)),
             pltpu.SemaphoreType.DMA((8,)),
         ],
@@ -1122,7 +1142,7 @@
         up_grad,
         down_grad,
         columns,
-        grads,
+        grads.reshape(outs.shape),
         outs,
         fqs,
         ends,

time: 113 us -> 112 us (level)
    pallas_call x1, Pallas kernels: 105 us -> 103 us  [square_call(): pl.pallas_call(square_kernel, out_shape=(shape((width, feats), bf16), sha...]
where the time goes in v4:
time: 112 us
  Pallas kernels  111 us (99%)
    pallas_call x1, Pallas kernels, square_call(): pl.pallas_call(square_kernel, out_shape=(shape((width, feats), bf16), sha...  103 us
    pallas_call x1, Pallas kernels, tail_call(): pl.pallas_call(tail_kernel, out_shape=tuple((shape(a.shape, a.dtype) for...  7.54 us

profile of v4, /device:TPU:27, one launch (start us, length us, event | category | flops | bytes accessed | tf_op | source)
XLA Modules:
  0.0 111.6 jit_solution(15542854965657414257)
XLA Ops:
  0.6 103.2 %shard_map.198 = (bf16[4096,256]{1,0:T(8,128)(2,1)}, bf16[4096,256]{1,0:T(8,128)(2,1)}, bf16[256,4096]{1,0:T(8,128)(2,1)}, bf16[4,160,1024]{2,1,0:T(8,128)(2,1)}...) custom-call(bf16[160,4096]{1,0:T(8,128)(2,1)} %raw_r_hbm.1, ...), custom_call_target="tpu_custom_call" | custom-call | flops 10737418240 | bytes 40000000 | tf_op jit(solution)/shard_map/pallas_call | solution.py:856
  103.9 7.5 %shard_map.199 = (bf16[4096,256]{1,0:T(8,128)(2,1)}, bf16[4096,256]{1,0:T(8,128)(2,1)}, bf16[256,4096]{1,0:T(8,128)(2,1)}, f32[1024,512]{1,0:T(8,128)}, bf16[160...) custom-call(bf16[4096,256]{1,0:T(8,128)(2,1)} %get-tuple-element.22.gate_in, ...), custom_call_target="tpu_custom_call" | custom-call | flops 671088640 | bytes 30000000 | tf_op jit(solution)/shard_map/pallas_call | solution.py:1090
